TPU v7x, 128 devices: a whole 4x4x4 slice. The times are simulated.
128 devices in a mesh: sp: 16 (over z, y), tp: 8 (over x, core).
Axes of the slice: x: 4, y: 4, z: 4, core: 2. Of those that a mesh axis runs over, the one named last changes fastest.
Arguments:
- inputs: bfloat16 [4096, 4096], P('sp', 'tp'), may hold values from -6 to 6
- input_norm_gain: bfloat16 [4096], replicated, may hold values from 0.099609375 to 1.8984375
- pooling_input_weight: bfloat16 [4096, 2048], P('sp', 'tp'), may hold values from -0.09375 to 0.09375
- query_weight: bfloat16 [4096, 2048], P('sp', 'tp'), may hold values from -0.09375 to 0.09375
- key_weight: bfloat16 [4096, 2048], P('sp', 'tp'), may hold values from -0.09375 to 0.09375
- value_weight: bfloat16 [4096, 2048], P('sp', 'tp'), may hold values from -0.09375 to 0.09375
- gate_weight: bfloat16 [4096, 2048], P('sp', 'tp'), may hold values from -0.09375 to 0.09375
- decay_weight: bfloat16 [4096, 16], replicated, may hold values from -0.25 to 0.25
- strength_weight: bfloat16 [4096, 16], replicated, may hold values from -0.09375 to 0.09375
- pooling_group_map: bfloat16 [16, 128, 128], P('tp'), may hold values from -0.5 to 0.5
- pooling_scale: float32 [2048], P('tp'), may hold values from 0.1 to 1.9
- head_log_decay: float32 [16], P('tp')
- decay_logit_bias: float32 [16], P('tp'), may hold values from -1 to 1
- write_logit_bias: float32 [16], P('tp')
- decay_position_factor: float32 [4096, 16], P('sp', 'tp'), may hold values from 0.28 to 3.25
- decay_position_offset: float32 [4096, 16], P('sp', 'tp'), may hold values from -0.7 to 0
- head_norm_gain: float32 [128], replicated, may hold values from 0.1 to 1.9
- pooling_output_weight: bfloat16 [2048, 4096], P('tp', 'sp'), may hold values from -0.125 to 0.125
- delta_output_weight: bfloat16 [2048, 4096], P('tp', 'sp'), may hold values from -0.125 to 0.125
Outputs:
- mixed_out: bfloat16 [4096, 4096], P('sp', 'tp')
All inputs are finite; a program needn't handle non-finite values.
Results may differ from a plain program's by a relative error of at most 0.02.
Values may be sent and summed in bfloat16 or wider, within the bound.
A program may use at most 128 MiB of HBM per device.

v0:
```python
import jax
import jax.numpy as jnp
from jax import lax
from jax.sharding import Mesh
from jax.sharding import PartitionSpec as P

HD = 128
PC = 128
BLK = 64
SP = ("sp_0", "sp_1")


epsilon = 1e-06
highest = lax.Precision.HIGHEST


def in_order(parts, dim):
    parts = jnp.moveaxis(parts, 0, dim)
    lengths = parts.shape
    return parts.reshape(*lengths[:dim], lengths[dim] * lengths[dim + 1], *lengths[dim + 2 :])


def from_everyone(shard, axis):
    peers = lax.axis_size(axis)
    return lax.all_to_all(
        jnp.broadcast_to(shard[None], (peers, *shard.shape)), axis, 0, 0, tiled=True
    )


def gather_directly(shard, axis, dim):
    return in_order(from_everyone(shard, axis), dim)


def in_one_piece(arrays, axis, dim, along):
    widths = [a.shape[along] for a in arrays]
    both = jnp.concatenate(arrays, axis=along)
    out = lax.all_gather(both, axis, axis=dim, tiled=True)
    return tuple(jnp.split(out, [sum(widths[:k]) for k in range(1, len(widths))], axis=along))


def shifted(value, axis, steps):
    count = lax.axis_size(axis)
    leading, last = (max(0, -steps), min(count, count - steps))
    return lax.ppermute(value, axis, [(source, source + steps) for source in range(leading, last)])


def filled_with(shard, identity):
    return jax.tree.map(
        lambda a, e: jnp.broadcast_to(jnp.asarray(e, a.dtype), a.shape), shard, identity
    )


def carried_in(shard, axes, combine, identity):
    before = start = filled_with(shard, identity)
    so_far = shard
    for axis in reversed(axes):
        peers, mine = (lax.axis_size(axis), lax.axis_index(axis))
        pieces = jax.tree.map(
            lambda part, kind: lax.all_gather(part.astype(kind), axis),
            so_far,
            jax.tree.map(lambda a: jnp.bfloat16 if a.dtype == jnp.float32 else a.dtype, shard),
        )
        inside, so_far = (start, start)
        for k in range(peers):
            passed = k < mine
            so_far = combine(
                so_far, jax.tree.map(lambda part, own: part[k].astype(own.dtype), pieces, shard)
            )
            inside = jax.tree.map(lambda new, old: jnp.where(passed, new, old), so_far, inside)
        before = combine(inside, before)
    return before


def unit_rows(matrix):
    return matrix * lax.rsqrt(jnp.sum(matrix * matrix, axis=-1, keepdims=True) + epsilon)


def pool_windows(first_group, group_count):
    group_ids = first_group + jnp.arange(group_count, dtype=jnp.int32)
    return 2 ** (1 + group_ids % 4)


def pool_branch(padded, windows, positions, pooling_group_map, pooling_scale):
    row_count = padded.shape[0] - 16
    window_sum = jnp.zeros(padded[16:].shape, jnp.float32)
    for lag_index in range(16):
        window_part = padded[16 - lag_index : 16 - lag_index + row_count]
        window_sum = (
            window_sum + window_part * (lag_index < windows).astype(jnp.float32)[None, :, None]
        )
    counts = jnp.minimum(positions[:, None] + 1, windows[None, :]).astype(jnp.float32)
    mixed = window_sum / counts[..., None] - padded[16:]
    projected = jnp.einsum(
        "tgc,gcd->tgd", mixed, pooling_group_map.astype(jnp.float32), precision=highest
    )
    return (projected.reshape(row_count, -1) * pooling_scale).astype(jnp.bfloat16)


def delta_rule_inputs(
    query_row_block,
    key_matrix_rows,
    value_row_block,
    decay_logits,
    write_logits,
    head_log_decay,
    decay_logit_bias,
    write_logit_bias,
    decay_position_factor,
    decay_position_offset,
):
    row_count = query_row_block.shape[0]
    head_count = head_log_decay.shape[0]

    def heads_of(matrix):
        return jax.nn.silu(matrix.astype(jnp.float32)).reshape(row_count, head_count, HD)

    query_matrix = unit_rows(heads_of(query_row_block)) * HD ** (-0.5)
    incoming_keys = unit_rows(heads_of(key_matrix_rows))
    value_matrix = heads_of(value_row_block)
    write_strength_rows = jax.nn.sigmoid(write_logits + write_logit_bias)
    decay_log_rows = (
        -jnp.exp(head_log_decay)
        * jax.nn.softplus(decay_logits + decay_logit_bias)
        * decay_position_factor
        + decay_position_offset
    )
    return (query_matrix, incoming_keys, value_matrix, write_strength_rows, decay_log_rows)


def block_terms(query_matrix, incoming_keys, value_matrix, write_strength_rows, decay_log_rows):
    length, head_count, head_depth = query_matrix.shape
    blocks = length // BLK

    def regroup(member):
        return member.reshape(blocks, BLK, head_count, -1).transpose(2, 0, 1, 3)

    query_matrix, incoming_keys, value_matrix = (
        regroup(query_matrix),
        regroup(incoming_keys),
        regroup(value_matrix),
    )
    write_strength_rows = write_strength_rows.reshape(blocks, BLK, head_count).transpose(2, 0, 1)
    running = jnp.cumsum(
        decay_log_rows.reshape(blocks, BLK, head_count).transpose(2, 0, 1), axis=-1
    )
    positions = jnp.arange(BLK)
    causal = positions[:, None] >= positions[None, :]
    strict = positions[:, None] > positions[None, :]
    spread = running[..., :, None] - running[..., None, :]
    decay_table = jnp.where(causal, jnp.exp(jnp.where(causal, spread, 0.0)), 0.0)
    weighted = incoming_keys * write_strength_rows[..., None]
    lower_part = jnp.where(
        strict,
        jnp.einsum("hnid,hnjd->hnij", weighted, incoming_keys, precision=highest) * decay_table,
        0.0,
    )
    system = lower_part + jnp.eye(BLK, dtype=jnp.float32)
    corrected = jax.scipy.linalg.solve_triangular(
        system, value_matrix * write_strength_rows[..., None], lower=True
    )
    erased = jax.scipy.linalg.solve_triangular(
        system, weighted * jnp.exp(running)[..., None], lower=True
    )
    scores = (
        jnp.einsum("hnid,hnjd->hnij", query_matrix, incoming_keys, precision=highest) * decay_table
    )
    query_decayed = query_matrix * jnp.exp(running)[..., None]
    block_total = running[..., -1]
    key_decayed = incoming_keys * jnp.exp(block_total[..., None] - running)[..., None]
    return (corrected, erased, query_decayed, key_decayed, scores, block_total)


def run_blocks(state_start, terms):

    def advance(state_now, pieces):
        corrected, erased, query_decayed, key_decayed, scores, block_total = pieces
        fresh_values = corrected - jnp.einsum("hcd,hde->hce", erased, state_now, precision=highest)
        output = jnp.einsum("hcd,hde->hce", query_decayed, state_now, precision=highest)
        output = output + jnp.einsum("hij,hje->hie", scores, fresh_values, precision=highest)
        state_now = state_now * jnp.exp(block_total)[:, None, None]
        state_now = state_now + jnp.einsum(
            "hcd,hce->hde", key_decayed, fresh_values, precision=highest
        )
        return (state_now, output)

    stacked = tuple((jnp.moveaxis(member, 1, 0) for member in terms))
    final_state, outputs = lax.scan(advance, state_start, stacked)
    blocks, head_count, block_rows, head_depth = outputs.shape
    return (
        final_state,
        outputs.transpose(0, 2, 1, 3).reshape(blocks * block_rows, head_count, head_depth),
    )


def compose_maps(terms):
    corrected, erased, query_decayed, key_decayed, scores, block_total = terms
    head_count, blocks, block_rows, head_depth = corrected.shape
    start_map = jnp.concatenate(
        [
            jnp.broadcast_to(
                jnp.eye(head_depth, dtype=jnp.float32), (head_count, head_depth, head_depth)
            ),
            jnp.zeros((head_count, head_depth, head_depth), jnp.float32),
        ],
        axis=-1,
    )

    def absorb(joined_map, pieces):
        corrected_block, erased_block, key_block, total_block = pieces
        target = jnp.concatenate([jnp.zeros_like(corrected_block), corrected_block], axis=-1)
        residue = target - jnp.einsum("hcd,hde->hce", erased_block, joined_map, precision=highest)
        updated = joined_map * jnp.exp(total_block)[:, None, None]
        updated = updated + jnp.einsum("hcd,hce->hde", key_block, residue, precision=highest)
        return (updated, None)

    stacked = tuple(
        (jnp.moveaxis(member, 1, 0) for member in (corrected, erased, key_decayed, block_total))
    )
    joined_map, unused = lax.scan(absorb, start_map, stacked)
    return (joined_map[..., :head_depth], joined_map[..., head_depth:])


def delta_finish(outputs, gate_rows, head_norm_gain):
    row_count, head_count, head_depth = outputs.shape
    scaled = (
        outputs
        * lax.rsqrt(jnp.mean(outputs * outputs, axis=-1, keepdims=True) + epsilon)
        * head_norm_gain
    )
    gated = scaled * jax.nn.silu(
        gate_rows.astype(jnp.float32).reshape(row_count, head_count, head_depth)
    )
    return gated.reshape(row_count, head_count * head_depth).astype(jnp.bfloat16)


def per_device(
    inputs,
    input_norm_gain,
    pooling_input_weight,
    query_weight,
    key_weight,
    value_weight,
    gate_weight,
    decay_weight,
    strength_weight,
    pooling_group_map,
    pooling_scale,
    head_log_decay,
    decay_logit_bias,
    write_logit_bias,
    decay_position_factor,
    decay_position_offset,
    head_norm_gain,
    pooling_output_weight,
    delta_output_weight,
):
    tok_rows = inputs.shape[0]
    gathered = gather_directly(inputs, "tp", 1)
    floats = gathered.astype(jnp.float32)
    normed = (
        floats
        * lax.rsqrt(jnp.mean(floats * floats, axis=-1, keepdims=True) + epsilon)
        * input_norm_gain.astype(jnp.float32)
    ).astype(jnp.bfloat16)
    head_count = head_log_decay.shape[0]
    head_first = lax.axis_index("tp") * head_count
    rate_weights = jnp.concatenate(
        [
            lax.dynamic_slice_in_dim(decay_weight, head_first, head_count, 1),
            lax.dynamic_slice_in_dim(strength_weight, head_first, head_count, 1),
        ],
        axis=1,
    )
    rate_rows = jnp.dot(normed, rate_weights, preferred_element_type=jnp.float32)
    decay_logits = rate_rows[:, :head_count]
    write_logits = rate_rows[:, head_count:]
    weights = (pooling_input_weight, query_weight, key_weight, value_weight, gate_weight)
    pieces = in_one_piece((weights[0], weights[1], weights[2], weights[3], weights[4]), SP, 0, 1)
    projected = tuple(
        (
            jnp.dot(normed, weight_piece, preferred_element_type=jnp.float32)
            for weight_piece in pieces
        )
    )
    pool_rows, query_row_block, key_matrix_rows, value_row_block, gate_rows = (
        member.astype(jnp.bfloat16) for member in projected
    )
    previous = shifted(pool_rows[tok_rows - 16 :], SP, 1)
    group_count = pooling_group_map.shape[0]
    padded = (
        jnp.concatenate([previous, pool_rows], axis=0)
        .astype(jnp.float32)
        .reshape(tok_rows + 16, group_count, PC)
    )
    positions = lax.axis_index(SP) * tok_rows + jnp.arange(tok_rows, dtype=jnp.int32)
    pool_out = pool_branch(
        padded,
        pool_windows(lax.axis_index("tp") * group_count, group_count),
        positions,
        pooling_group_map,
        pooling_scale,
    )
    query_matrix, incoming_keys, value_matrix, write_strength_rows, decay_log_rows = (
        delta_rule_inputs(
            query_row_block,
            key_matrix_rows,
            value_row_block,
            decay_logits,
            write_logits,
            head_log_decay,
            decay_logit_bias,
            write_logit_bias,
            decay_position_factor,
            decay_position_offset,
        )
    )
    terms = block_terms(
        query_matrix, incoming_keys, value_matrix, write_strength_rows, decay_log_rows
    )
    transition = compose_maps(terms)
    identity = (
        jnp.broadcast_to(jnp.eye(HD, dtype=jnp.float32), (head_count, HD, HD)),
        jnp.zeros((head_count, HD, HD), jnp.float32),
    )

    def chain_maps(earlier, later):
        joined_map = jnp.einsum("hij,hjk->hik", later[0], earlier[0], precision=highest)
        joined_add = jnp.einsum("hij,hjk->hik", later[0], earlier[1], precision=highest) + later[1]
        return (joined_map, joined_add)

    prefix = carried_in(transition, SP, chain_maps, identity)
    state_in = prefix[1]
    unused_state, outputs = run_blocks(state_in, terms)
    delta_out = delta_finish(outputs, gate_rows, head_norm_gain)
    both_out = jnp.concatenate([pool_out, delta_out], axis=1)
    out_weights = jnp.concatenate([pooling_output_weight, delta_output_weight], axis=0)
    partial_value = jnp.dot(
        both_out,
        lax.all_gather(out_weights, SP, axis=1, tiled=True),
        preferred_element_type=jnp.float32,
    )
    summed = lax.psum_scatter(
        partial_value.astype(jnp.bfloat16), "tp", scatter_dimension=1, tiled=True
    )
    return summed


def solution(mesh):
    torus = Mesh(mesh.devices.reshape(4, 4, mesh.shape["tp"]), ("sp_0", "sp_1", "tp"))
    in_specs = (
        P(SP, "tp"),
        P(),
        P(SP, "tp"),
        P(SP, "tp"),
        P(SP, "tp"),
        P(SP, "tp"),
        P(SP, "tp"),
        P(),
        P(),
        P("tp", None, None),
        P("tp"),
        P("tp"),
        P("tp"),
        P("tp"),
        P(SP, "tp"),
        P(SP, "tp"),
        P(),
        P("tp", SP),
        P("tp", SP),
    )
    out_specs = P(SP, "tp")
    return jax.shard_map(
        per_device, mesh=torus, in_specs=in_specs, out_specs=out_specs, check_vma=False
    )
```

profile of v0, /device:TPU:1, one launch (start us, length us, event | category | flops | bytes accessed | tf_op | source)
XLA Modules:
  0.0 288.1 jit_solution(10694764772919519181)
XLA Ops:
  12.2 1.4 broadcast_in_dim.41
  13.7 5.9 %all-to-all-start = ((bf16[8,256,512]{1,2,0:T(8,128)(2,1)}), bf16[8,256,512]{1,2,0:T(8,128)(2,1)S(1)}, u32[]{:S(2)}, u32[]{:S(2)}) async-start(bf16[8,256,512]{1,2,0:T(8,128)(2,1)} %broadcast_in_dim.41), calls=%async_computation | async-start | bytes 4194304 | tf_op jit(solution)/shard_map/all_to_all | solution.py:25
  28.8 17.0 %all-to-all-done = bf16[8,256,512]{1,2,0:T(8,128)(2,1)S(1)} async-done(((bf16[8,256,512]{1,2,0:T(8,128)(2,1)}), bf16[8,256,512]{1,2,0:T(8,128)(2,1)S(1)}, u32[]{:S(2)}, u32[]{:S(2)}) %all-to-all-start) | async-done | bytes 2097184 | tf_op jit(solution)/shard_map/all_to_all | solution.py:25
  47.1 1.9 fusion.23
  52.8 42.9 %all-gather.7.cloned.1.call-done = bf16[4096,1280]{1,0:T(8,128)(2,1)} async-done(((bf16[256,1280]{1,0:T(8,128)(2,1)}), bf16[4096,1280]{1,0:T(8,128)(2,1)}) %all-gather.7.cloned.1.call-update) | async-done | bytes 10485776 | tf_op jit(solution)/shard_map/all_gather | solution.py:37
  95.7 2.3 fusion.39
  98.7 3.7 %collective-permute-start = (bf16[16,256]{1,0:T(8,128)(2,1)}, bf16[16,256]{1,0:T(8,128)(2,1)}, u32[]{:S(2)}, u32[]{:S(2)}) collective-permute-start(bf16[16,256]{1,0:T(8,128)(2,1)} %slice.239), channel_id=1, source_target_pairs={{0,8},{8,16},{16,24},{24,32},{32,40},{40,48},{48,56},{56,64},{64,7... | collective-permute-start | bytes 24584 | tf_op jit(solution)/shard_map/ppermute | solution.py:44
  102.4 2.6 bitcast_reduce_fusion
  106.7 2.6 bitcast_reduce_fusion.1
  109.9 1.5 fusion.38
  111.4 39.3 %custom-call.4 = f32[2,4,1,64,64]{3,4,2,1,0:T(8,128)S(1)} custom-call(f32[2,4,1,64,64]{4,3,2,1,0:T(8,128)S(1)} %fusion.38), custom_call_target="InvertDiagBlocksLowerTriangular" | custom-call | tf_op jit(solution)/shard_map/jit(_solve_triangular)/vmap(vmap())/triangular_solve | solution.py:158
  151.5 1.5 convolution_bitcast_fusion.1
  153.0 3.2 %divide_multiply_fusion.1 = f32[256,256]{0,1:T(8,128)} fusion(bf16[256,4096]{0,1:T(8,128)(2,1)S(1)} %fusion.23, bf16[4096,1280]{1,0:T(8,128)(2,1)} %all-gather.7.cloned.1.call-done), kind=kOutput, calls=%fused_computation.168 | convolution fusion | flops 537264128 | bytes 4456448 | tf_op jit(solution)/shard_map/dot_general | solution.py:281
  156.3 1.2 reshape.398
  158.3 1.7 convolution_bitcast_fusion.2
  160.3 5.8 %while.22 = (s32[]{:T(128)}, f32[2,128,256]{2,1,0:T(8,128)S(1)}, f32[4,2]{1,0:T(4,128)}, f32[4,2,64,128]{3,2,1,0:T(8,128)S(1)}, f32[4,2,64,128]{3,2,1,0:T(8,128)S(1)}, /*index=5*/f32[4,2,64,128]{3,2,1,0:T(8,128)S(1)}, s32[]{:T(128)}) while((s32[]{:T(128)}, f32[2,128,256]{2,1,0:T(8,128)S(1)}, f32[4,2]{1,0:T(4,128)}, ...), condition=%wide.region_4.6_spmd, body=%wide.region_3.5_spmd.sunk | while | flops 100827136 | bytes 1376877 | solution.py:219
  166.1 9.8 %all-gather = bf16[8,128,128]{2,1,0:T(8,128)(2,1)S(1)} all-gather(bf16[2,128,128]{2,1,0:T(8,128)(2,1)S(1)} %get-tuple-element.209), channel_id=2, replica_groups=mesh['sp_0'=4,'sp_1'=4,'tp'=8] {'sp_1'}, dimensions={0}, use_global_device_ids=true | all-gather | bytes 327680 | tf_op jit(solution)/shard_map/all_gather | solution.py:59
  175.9 9.4 %all-gather.2 = bf16[8,128,128]{2,1,0:T(8,128)(2,1)S(1)} all-gather(bf16[2,128,128]{2,1,0:T(8,128)(2,1)S(1)} %get-tuple-element.208), channel_id=4, replica_groups=mesh['sp_0'=4,'sp_1'=4,'tp'=8] {'sp_1'}, dimensions={0}, use_global_device_ids=true | all-gather | bytes 327680 | tf_op jit(solution)/shard_map/all_gather | solution.py:59
  186.3 9.8 %all-gather.3 = bf16[8,128,128]{2,1,0:T(8,128)(2,1)S(1)} all-gather(bf16[2,128,128]{2,1,0:T(8,128)(2,1)S(1)} %get-tuple-element.218), channel_id=5, replica_groups=mesh['sp_0'=4,'sp_1'=4,'tp'=8] {'sp_0'}, dimensions={0}, use_global_device_ids=true | all-gather | bytes 327680 | tf_op jit(solution)/shard_map/all_gather | solution.py:59
  196.9 10.0 %all-gather.1 = bf16[8,128,128]{2,1,0:T(8,128)(2,1)S(1)} all-gather(bf16[2,128,128]{2,1,0:T(8,128)(2,1)S(1)} %get-tuple-element.216), channel_id=3, replica_groups=mesh['sp_0'=4,'sp_1'=4,'tp'=8] {'sp_0'}, dimensions={0}, use_global_device_ids=true | all-gather | bytes 327680 | tf_op jit(solution)/shard_map/all_gather | solution.py:59
  208.7 1.3 bitcast_multiply_fusion.20
  210.0 1.3 fusion.34
  211.6 16.5 %while.23 = (s32[]{:T(128)}, f32[2,128,128]{2,1,0:T(8,128)S(1)}, f32[4,2,64,128]{3,2,1,0:T(8,128)}, f32[4,2]{1,0:T(4,128)}, f32[4,2,64,128]{3,2,1,0:T(8,128)S(1)...) while((s32[]{:T(128)}, f32[2,128,128]{2,1,0:T(8,128)S(1)}, ...), condition=%wide.region_7.9_spmd, body=%wide.region_6.8_spmd.sunk | while | flops 88178688 | bytes 1378945 | solution.py:187
  212.9 1.7 fusion.285
  217.1 1.7 fusion.285
  221.2 1.7 fusion.285
  225.3 1.7 fusion.285
  228.1 1.1 multiply_reduce_fusion.1
  229.2 1.2 copy.267
  230.8 2.6 fusion.124
  235.8 4.8 %convolution_convert_fusion = bf16[256,4096]{1,0:T(8,128)(2,1)} fusion(bf16[512,4096]{1,0:T(8,128)(2,1)} %all-gather.9.cloned.1.call-done, bf16[256,256]{0,1:T(8,128)(2,1)S(1)} %fusion.124, bf16[256,256]{0,1:T(8,128)(2,1)S(1)} %fusion.121), kind=kOutput, calls=%fused_computation.32 | convolution fusion | flops 1075314688 | bytes 6553600 | tf_op jit(solution)/shard_map/dot_general | solution.py:337
  240.7 40.9 %reduce-scatter.2.cloned.1.call-done = bf16[256,512]{1,0:T(8,128)(2,1)} async-done(((bf16[256,4096]{1,0:T(8,128)(2,1)}), bf16[256,512]{1,0:T(8,128)(2,1)}) %reduce-scatter.2.cloned.1.call-update) | async-done | bytes 262160 | tf_op jit(solution)/shard_map/reduce_scatter | solution.py:342
  (201 shorter events, 46.1 us)
Async XLA Ops:
  6.5 228.1 %copy-start = (bf16[2,128,128]{2,1,0:T(8,128)(2,1)S(1)}, bf16[2,128,128]{2,1,0:T(8,128)(2,1)}, u32[]{:S(2)}) copy-start(bf16[2,128,128]{2,1,0:T(8,128)(2,1)} %param.34) | copy-start | bytes 196612
  6.5 5.5 %copy-start.7 = (bf16[256,512]{1,0:T(8,128)(2,1)S(1)}, bf16[256,512]{1,0:T(8,128)(2,1)}, u32[]{:S(2)}) copy-start(bf16[256,512]{1,0:T(8,128)(2,1)} %param.25) | copy-start | bytes 786436
  6.5 89.2 %all-gather.7.cloned.1.call-start = ((), (), s32[]{:S(2)}) async-start(), calls=%async_computation.2 | async-start | bytes 11141120 | tf_op jit(solution)/shard_map/all_gather | solution.py:37
  11.2 0.9 copy-start.5
  13.6 6.0 %copy-start.10 = (bf16[256,256]{1,0:T(8,128)(2,1)S(1)}, bf16[256,256]{1,0:T(8,128)(2,1)}, u32[]{:S(2)}) copy-start(bf16[256,256]{1,0:T(8,128)(2,1)} %param.43) | copy-start | bytes 393220
  13.7 6.0 %copy-start.11 = (bf16[256,256]{1,0:T(8,128)(2,1)S(1)}, bf16[256,256]{1,0:T(8,128)(2,1)}, u32[]{:S(2)}) copy-start(bf16[256,256]{1,0:T(8,128)(2,1)} %param.42) | copy-start | bytes 393220
  13.7 9.8 %copy-start.14 = (bf16[4096]{0:T(1024)(128)(2,1)S(1)}, bf16[4096]{0:T(1024)(128)(2,1)}, u32[]{:S(2)}) copy-start(bf16[4096]{0:T(1024)(128)(2,1)} %param.26) | copy-start | bytes 24580
  13.7 12.9 %copy-start.37 = (f32[2]{0:T(128)S(1)}, f32[2]{0:T(128)}, u32[]{:S(2)}) copy-start(f32[2]{0:T(128)} %param.36) | copy-start | bytes 28
  13.7 12.9 %copy-start.38 = (f32[128]{0:T(128)S(1)}, f32[128]{0:T(128)}, u32[]{:S(2)}) copy-start(f32[128]{0:T(128)} %param.41) | copy-start | bytes 1540
  13.7 32.1 %all-to-all-start = ((bf16[8,256,512]{1,2,0:T(8,128)(2,1)}), bf16[8,256,512]{1,2,0:T(8,128)(2,1)S(1)}, u32[]{:S(2)}, u32[]{:S(2)}) async-start(bf16[8,256,512]{1,2,0:T(8,128)(2,1)} %broadcast_in_dim.41), calls=%async_computation | async-start | bytes 4194304 | tf_op jit(solution)/shard_map/all_to_all | solution.py:25
  19.6 216.2 %all-gather.9.cloned.1.call-start = ((), (), s32[]{:S(2)}) async-start(), calls=%async_computation.3 | async-start | bytes 4456448 | tf_op jit(solution)/shard_map/all_gather | solution.py:339
  20.4 261.2 %reduce-scatter.2.cloned.1.call-start = ((), (), s32[]{:S(2)}) async-start(), calls=%async_computation.4 | async-start | bytes 2359296 | tf_op jit(solution)/shard_map/reduce_scatter | solution.py:342
  45.8 1.3 copy-start.1
  49.1 0.7 copy-start.15
  49.1 0.7 copy-start.16
  49.1 0.7 copy-start.35
  98.7 134.7 %collective-permute-start = (bf16[16,256]{1,0:T(8,128)(2,1)}, bf16[16,256]{1,0:T(8,128)(2,1)}, u32[]{:S(2)}, u32[]{:S(2)}) collective-permute-start(bf16[16,256]{1,0:T(8,128)(2,1)} %slice.239), channel_id=1, source_target_pairs={{0,8},{8,16},{16,24},{24,32},{32,40},{40,48},{48,56},{56,64},{64,7... | collective-permute-start | bytes 24584 | tf_op jit(solution)/shard_map/ppermute | solution.py:44
  150.8 0.7 copy-start.4
  196.6 11.7 %copy-start.2 = (f32[4,64,2,128]{3,2,1,0:T(2,128)S(1)}, f32[4,64,2,128]{3,2,1,0:T(2,128)}, u32[]{:S(2)}) copy-start(f32[4,64,2,128]{3,2,1,0:T(2,128)} %reshape.342) | copy-start | bytes 786436
  196.6 11.7 %copy-start.3 = (f32[256,2]{1,0:T(8,128)S(1)}, f32[256,2]{1,0:T(8,128)}, u32[]{:S(2)}) copy-start(f32[256,2]{1,0:T(8,128)} %copy.266) | copy-start | bytes 6148
  196.9 11.8 %copy-start.6 = (f32[4,2,64]{1,2,0:T(8,128)S(1)}, f32[4,2,64]{1,2,0:T(8,128)}, u32[]{:S(2)}) copy-start(f32[4,2,64]{1,2,0:T(8,128)} %copy.247) | copy-start | bytes 6148
  207.0 2.9 %copy-start.12 = (pred[64,64]{1,0:T(8,128)(4,1)S(1)}, pred[64,64]{1,0:T(8,128)(4,1)}, u32[]{:S(2)}) copy-start(pred[64,64]{1,0:T(8,128)(4,1)} %get-tuple-element.240) | copy-start | bytes 12292
  211.6 19.2 %copy-start.18 = (f32[256]{0:T(256)S(1)}, f32[256]{0:T(256)}, u32[]{:S(2)}) copy-start(f32[256]{0:T(256)} %broadcast_bitcast_fusion) | copy-start | bytes 3076
  230.8 2.6 copy-start.9
  234.1 0.7 copy-start.13
  234.1 0.7 copy-start.19
  234.2 0.7 copy-start.28
  234.2 0.7 copy-start.29
  234.2 0.7 copy-start.30
  234.3 0.7 copy-start.33
  234.3 0.7 copy-start.34
  235.0 0.7 copy-start.17
  (12 other events, 8.0 us)
Sparse Core Ops, SparseCore 0:
  12.2 83.4 all-gather.6
  97.8 56.9 all-gather.8
  240.8 40.6 reduce-scatter.1
where the time goes:
time: 292 us; the launch traced here: 288 us
  waiting for transfers between devices  101 us (35%)
  other arithmetic  53.7 us (18%)
  matrix products  41.6 us (14%)
  blocking collectives  39 us (13%)
  local copies, waits for them, and re-layouts  29 us (10%)
  between operations  13.9 us (5%)
  starting transfers between devices  9.67 us (3%)
    all_gather x1, waiting for transfers between devices, in_one_piece(): out = lax.all_gather(both, axis, axis=dim, tiled=True)  42.9 us
    reduce_scatter x1, waiting for transfers between devices, per_device(): lax.psum_scatter(partial_value.astype(jnp.bfloat16), 'tp', scatter_dimens...  40.9 us
    another operation x2, other arithmetic, block_terms(): jax.scipy.linalg.solve_triangular(system, value_matrix * write_strength_r...  39.9 us
    all_gather x4, blocking collectives, carried_in(): lax.all_gather(part.astype(kind), axis)  39 us
    all_to_all x1, waiting for transfers between devices, from_everyone(): lax.all_to_all(jnp.broadcast_to(shard[None], (peers, *shard.shape)), axis...  17 us
    dot_general x5, matrix products, per_device(): jnp.dot(normed, weight_piece, preferred_element_type=jnp.float32)  13.3 us
    unnamed x84, local copies, waits for them, and re-layouts  7.15 us
    dot_general x4, matrix products, advance(): jnp.einsum('hij,hje->hie', scores, fresh_values, precision=highest)  6.67 us
  transfers between devices with their start and end apart: 5, of which 3 were waited for; matrix products, arithmetic and copies ran while one was open for 39% of the time, Pallas kernels for 0%

commit v1 on v0

v1 whole, which is shorter than its diff:
```python
import functools

import jax
import jax.numpy as jnp
from jax import lax
from jax.experimental import pallas as pl
from jax.experimental.pallas import tpu as pltpu
from jax.sharding import PartitionSpec as P

MESH = pl.DeviceIdType.MESH
F32 = jnp.float32
BF16 = jnp.bfloat16
HD = 128
EPS = 1e-06
HIGHEST = lax.Precision.HIGHEST


def dot(a, b, dims=((1,), (0,)), precision=None):
    return lax.dot_general(
        a, b, (dims, ((), ())), precision=precision, preferred_element_type=F32
    )


def iota(shape, dim):
    return lax.broadcasted_iota(jnp.int32, shape, dim)


def silu(a):
    return a * jax.nn.sigmoid(a)


def unit(a):
    return a * lax.rsqrt(jnp.sum(a * a, axis=-1, keepdims=True) + EPS)


def kernel(
    x_in, wp_in, wq_in, wk_in, wv_in, wg_in, op_in, od_in, pk_in, pm_in,
    pk_v, dw_v, sw_v,
    out_ref,
    xbuf, wbuf, wo, packb, pmb, xg, acc, ssq,
    stc, stz_src, stz, pad, pool_src, delta_src, prev_src, ap, ad,
    rs2, rsp, rsm, rl, rin, o0, pmx, kw0_s, b0_s, keep_s, low_s, inv_s, up_s, down_s, state_s,
    x_rs, w_rs, wo_rs, pk_rs, pm_rs, st_rs, stz_rs, prev_rs, ap_rs, ad_rs, rs_rs,
    x_ss, xf_ss, w_ss, wf_ss, wo_ss, wof_ss, pk_ss, pm_ss, st_ss, stz_ss, prev_ss,
    ap_ss, ad_ss, apf_ss, adf_ss, rs_ss,
):
    sp, tp = lax.axis_index("sp"), lax.axis_index("tp")
    z, y = lax.div(sp, 4), lax.rem(sp, 4)
    x, c = lax.div(tp, 2), lax.rem(tp, 2)
    kh = lax.div(y, 2)
    yodd = lax.rem(y, 2)
    home = c == kh
    away = jnp.logical_not(home)

    def mod4(a):
        return lax.rem(a + 8, 4)

    def dev(zz, yy, xx, cc):
        return (4 * zz + yy, 2 * xx + cc)

    zp, zm, z2 = mod4(z + 1), mod4(z - 1), mod4(z + 2)
    yp, ym = mod4(y + 1), mod4(y - 1)
    xp, xm, x2 = mod4(x + 1), mod4(x - 1), mod4(x + 2)
    me_z, me_y, me_x = z, y, x
    partner = dev(z, y, x, 1 - c)

    ends = []

    def remote(src, dst, ssem, rsem, to, cond=None):
        def make():
            return pltpu.make_async_remote_copy(
                src_ref=src, dst_ref=dst, send_sem=ssem, recv_sem=rsem,
                device_id=to, device_id_type=MESH,
            )

        if cond is None:
            make().start()
            ends.append(lambda: make().wait_send())
        else:
            @pl.when(cond)
            def _():
                make().start()

            def end():
                @pl.when(cond)
                def _():
                    make().wait_send()

            ends.append(end)

    def arrived(ref, sem):
        pltpu.make_async_copy(ref, ref, sem).wait()

    barrier = pltpu.get_barrier_semaphore()
    peers = [partner]
    for d in (1, 2, 3):
        for cc in (0, 1):
            peers.append(dev(mod4(z + d), y, x, cc))
            peers.append(dev(z, mod4(y + d), x, cc))
            peers.append(dev(z, y, mod4(x + d), cc))
    for to in peers:
        pl.semaphore_signal(barrier, inc=1, device_id=to, device_id_type=MESH)
    pl.semaphore_wait(barrier, len(peers))

    def xslot(yy, xx, cc):
        return xbuf.at[2 * xx + cc, pl.ds(256 * lax.rem(yy, 2), 256), :]

    def xsem(yy, xx, cc):
        return x_rs.at[8 * lax.rem(yy, 2) + 2 * xx + cc]

    def wslot(zz, yy, r):
        return wbuf.at[2 * (4 * zz + yy) + r, :, pl.ds(0, 640)]

    def wsem(zz, yy, r):
        return w_rs.at[2 * (4 * zz + yy) + r]

    def woslot(zz, yy, cc):
        return wo.at[zz, 2 * lax.rem(yy, 2) + cc]

    def wosem(zz, yy, cc):
        return wo_rs.at[4 * zz + 2 * lax.rem(yy, 2) + cc]

    own = xslot(y, x, c)
    own_sem = xsem(y, x, c)
    remote(x_in, own, x_ss.at[0], own_sem, dev(z, y, xp, kh))
    remote(x_in, own, x_ss.at[1], own_sem, dev(z, y, xm, kh))
    remote(x_in, own, x_ss.at[2], own_sem, dev(z, yp, x, kh))
    remote(x_in, own, x_ss.at[3], own_sem, dev(z, ym, x, kh))
    remote(x_in, own, x_ss.at[4], own_sem, partner, away)

    @pl.when(home)
    def _():
        pltpu.make_async_copy(x_in, own, own_sem).start()

    wo_own = woslot(z, y, c)
    for half, ref in enumerate((op_in, od_in)):
        part = wo_own.at[pl.ds(256 * half, 256), :]
        for i, zz in enumerate((zp, zm)):
            remote(ref, part, wo_ss.at[2 * half + i], wosem(z, y, c), dev(zz, y, x, kh))
        remote(ref, part, wo_ss.at[4 + half], wosem(z, y, c), partner, away)

        @pl.when(home)
        def _(ref=ref, part=part):
            pltpu.make_async_copy(ref, part, wosem(z, y, c)).start()

    for j in (0, 1):
        head_y = 2 * c + j
        for r in (0, 1):
            self_here = jnp.logical_and(head_y == y, c == r)
            for n, ref in enumerate((wp_in, wq_in, wk_in, wv_in, wg_in)):
                src = ref.at[pl.ds(128 * r, 128), pl.ds(128 * j, 128)]
                dst = wbuf.at[2 * sp + r, :, pl.ds(128 * n, 128)]
                remote(
                    src, dst, w_ss.at[5 * (2 * j + r) + n], wsem(z, y, r),
                    dev(z, head_y, x, r), jnp.logical_not(self_here),
                )

                @pl.when(self_here)
                def _(src=src, dst=dst, r=r):
                    pltpu.make_async_copy(src, dst, wsem(z, y, r)).start()

    for j in (0, 1):
        head_y = 2 * c + j
        self_here = jnp.logical_and(head_y == y, home)
        src = pk_in.at[pl.ds(8, 16), :]
        dst = packb.at[yodd]
        remote(
            src, dst, pk_ss.at[j], pk_rs.at[yodd], dev(z, head_y, x, kh),
            jnp.logical_not(self_here),
        )

        @pl.when(self_here)
        def _(src=src, dst=dst):
            pltpu.make_async_copy(src, dst, pk_rs.at[yodd]).start()

    remote(pm_in.at[yodd], pmb, pm_ss.at[0], pm_rs.at[0], partner, home)

    @pl.when(home)
    def _():
        pltpu.make_async_copy(pm_in.at[yodd], pmb, pm_rs.at[0]).start()

    head = 4 * x + y
    row16, col16 = iota((16, 128), 0), iota((16, 128), 1)
    pick_d = jnp.logical_and(row16 == head, col16 == 0).astype(BF16)
    pick_s = jnp.logical_and(row16 == head, col16 == 1).astype(BF16)

    def fill(i, carry):
        rows = pl.ds(pl.multiple_of(128 * i, 128), 128)
        both = dot(dw_v[rows, :], pick_d) + dot(sw_v[rows, :], pick_s)
        wbuf[i, :, 640:768] = both.astype(BF16)
        return carry

    lax.fori_loop(0, 32, fill, 0)

    def w_first(d, n):
        yy = mod4(me_y + d)
        slot = wslot(me_z, yy, c)
        arrived(slot, wsem(me_z, yy, c))
        remote(slot, slot, wf_ss.at[n], wsem(me_z, yy, c), dev(zp, y, x, c))
        remote(slot, slot, wf_ss.at[n + 1], wsem(me_z, yy, c), dev(zm, y, x, c))
        remote(slot, slot, wf_ss.at[n + 2], wsem(me_z, yy, c), partner)

    def w_later(zz, d, n, to_z=None):
        yy = mod4(me_y + d)
        slot = wslot(zz, yy, c)
        arrived(slot, wsem(zz, yy, c))
        if to_z is not None:
            remote(slot, slot, wf_ss.at[n + 1], wsem(zz, yy, c), dev(to_z, y, x, c))
        remote(slot, slot, wf_ss.at[n], wsem(zz, yy, c), partner)

    yn = 2 * c + 1 - yodd
    yo = 2 * c + yodd
    from_below = mod4(yn + 1) == y
    relay_c = jnp.where(from_below, 0, 1)
    y_next = jnp.where(from_below, yp, ym)

    w_first(0, 0)
    for cc in (0, 1):
        slot = xslot(yn, x, cc)
        arrived(slot, xsem(yn, x, cc))
        remote(slot, slot, xf_ss.at[2 * cc], xsem(yn, x, cc), dev(z, y, xp, c))
        remote(slot, slot, xf_ss.at[2 * cc + 1], xsem(yn, x, cc), dev(z, y, xm, c))
    slot = xslot(yn, x, relay_c)
    remote(slot, slot, xf_ss.at[4], xsem(yn, x, relay_c), dev(z, y_next, x, c))
    w_first(1, 3)
    w_first(3, 6)
    for cc in (0, 1):
        slot = xslot(yo, x, cc)
        arrived(slot, xsem(yo, x, cc))
        remote(slot, slot, xf_ss.at[5 + 2 * cc], xsem(yo, x, cc), dev(z, y, xp, c), away)
        remote(slot, slot, xf_ss.at[6 + 2 * cc], xsem(yo, x, cc), dev(z, y, xm, c), away)
    w_first(2, 9)

    yf = jnp.where(home, yo, yn)
    yl = jnp.where(home, yn, yo)
    n = 9
    for yy in (yf, yl):
        for xx, cc, to_x in ((xm, 0, xp), (xp, 1, xm)):
            slot = xslot(yy, xx, cc)
            arrived(slot, xsem(yy, xx, cc))
            remote(slot, slot, xf_ss.at[n], xsem(yy, xx, cc), dev(z, y, to_x, c))
            n += 1

    def wo_home(zz, cc, n, to_z=None):
        @pl.when(home)
        def _():
            slot = woslot(zz, me_y, cc)
            arrived(slot, wosem(zz, me_y, cc))

        slot = woslot(zz, me_y, cc)
        sem = wosem(zz, me_y, cc)
        if to_z is not None:
            remote(slot, slot, wof_ss.at[n], sem, dev(to_z, y, x, c), home)
        remote(slot, slot, wof_ss.at[n + 1], sem, dev(z, yp, x, c), home)
        remote(slot, slot, wof_ss.at[n + 2], sem, dev(z, ym, x, c), home)

    wo_home(z, 0, 0)
    wo_home(z, 1, 3)
    wo_home(zm, 0, 6, zp)
    wo_home(zp, 1, 9, zm)

    n = 12
    for d in (0, 1, 3, 2):
        w_later(zm, d, n, zp if d in (0, 2) else None)
        w_later(zp, d, n + 2, zm if d in (1, 3) else None)
        n += 4

    wo_home(zm, 1, 12)
    wo_home(zp, 0, 15)
    wo_home(z2, 0, 18)
    wo_home(z2, 1, 21)

    for d in (0, 1, 3, 2):
        w_later(z2, d, n)
        n += 1

    for yy in (yn, yo):
        for xx, cc in ((xm, 1), (xp, 0), (x2, 0), (x2, 1)):
            arrived(xslot(yy, xx, cc), xsem(yy, xx, cc))
    for zz in (z, zp, zm, z2):
        for d in (0, 1, 2, 3):
            yy = mod4(y + d)
            arrived(wslot(zz, yy, 1 - c), wsem(zz, yy, 1 - c))

    ssq[...] = jnp.zeros_like(ssq)
    acc[...] = jnp.zeros_like(acc)

    def project(i, carry):
        gain = pk_v[pl.ds(i, 1), :]
        for b in range(4):
            rows = slice(128 * b, 128 * b + 128)
            v = xbuf[i, rows, :].astype(F32)
            sq = v * v
            ssq[rows, :] += (
                (sq[:, 0:128] + sq[:, 128:256]) + (sq[:, 256:384] + sq[:, 384:512])
            )
            xg[rows, :] = (v * gain).astype(BF16)
        acc[...] += dot(xg[...], wbuf[pl.ds(4 * i, 4)].reshape(512, 768))
        return carry

    lax.fori_loop(0, 8, project, 0)

    def wo_away_pump(zs, n):
        for zz in zs:
            for cc in (0, 1):
                arrived(woslot(zz, yn, cc), wosem(zz, yn, cc))
            slot = woslot(zz, yn, relay_c)
            remote(slot, slot, wof_ss.at[n], wosem(zz, yn, relay_c), dev(z, y_next, x, c))
            n += 1

    wo_away_pump((z, zm), 24)

    for b in (0, 1):
        arrived(packb.at[b], pk_rs.at[b])
    arrived(pmb, pm_rs.at[0])

    ii, jj = iota((256, 256), 0), iota((256, 256), 1)
    diff = jnp.bitwise_xor(ii, jj)
    lower = ii > jj
    causal = ii >= jj
    upto = (ii <= jj).astype(F32)
    eye = (ii == jj).astype(F32)

    def row_scale(b):
        total = jnp.sum(ssq[256 * b : 256 * b + 256, :], axis=-1, keepdims=True)
        return lax.rsqrt(total * (1.0 / 4096.0) + EPS)

    scale = [row_scale(0), row_scale(1)]

    for b in (0, 1):
        pad[16 + 256 * b : 272 + 256 * b, :] = acc[256 * b : 256 * b + 256, 0:128] * scale[b]
    prev_src[...] = pad[512:528, :].astype(BF16)
    prev_to = dev(jnp.where(c == 0, z, zp), y, x, 1 - c)
    last = jnp.logical_and(z == 3, c == 1)
    first = jnp.logical_and(z == 0, c == 0)
    prev_dst = ap.at[pl.ds(256, 16), pl.ds(0, 128)]
    remote(prev_src, prev_dst, prev_ss.at[0], prev_rs.at[0], prev_to, jnp.logical_not(last))

    heads = []
    for b in (0, 1):
        rows = slice(256 * b, 256 * b + 256)
        s = scale[b]
        q = unit(silu(acc[rows, 128:256] * s)) * HD ** (-0.5)
        k = unit(silu(acc[rows, 256:384] * s))
        v = silu(acc[rows, 384:512] * s)
        rate = acc[rows, 640:768] * s
        table = packb[b]
        pick = lambda r: jnp.where(yodd == 0, table[r : r + 1, 0:256], table[r + 1 : r + 2, 0:256])
        factor, offset, hld, dlb, wlb = (pick(r) for r in (0, 2, 4, 6, 8))
        pre = rate.T[0:1, :] + dlb
        soft = jnp.maximum(pre, 0.0) + jnp.log1p(jnp.exp(-jnp.abs(pre)))
        log_decay = -jnp.exp(hld) * soft * factor + offset
        run_row = dot(jnp.broadcast_to(log_decay, (8, 256)), upto, precision=HIGHEST)[0:1, :]
        run = jnp.broadcast_to(run_row, (128, 256)).T
        beta = jax.nn.sigmoid(rate[:, 1:2] + wlb[:, 0:1])
        spread = jnp.concatenate([run, run], axis=1) - run_row
        decay = jnp.where(causal, jnp.exp(jnp.where(causal, spread, 0.0)), 0.0)
        k16, q16 = k.astype(BF16), q.astype(BF16)
        low = jnp.where(lower, dot(k16, k16, ((1,), (1,))) * (decay * beta), 0.0)
        scores = (dot(q16, k16, ((1,), (1,))) * decay).astype(BF16)
        inverse = eye - jnp.where(diff == 1, low, 0.0)
        grown = jnp.exp(run)
        kb = k * beta
        low_s[b] = low
        inv_s[b] = inverse
        heads.append(dict(q=q, k=k, v=v, scores=scores, run=run, grown=grown, kb=kb, beta=beta))

    for level in range(1, 8):
        mask = jnp.right_shift(diff, level) == 1
        mids = []
        for b in (0, 1):
            off = jnp.where(mask, low_s[b], 0.0).astype(BF16)
            mids.append(dot(off, inv_s[b].astype(BF16)).astype(BF16))
        for b, mid in enumerate(mids):
            inv_s[b] = inv_s[b] - dot(inv_s[b].astype(BF16), mid)

    maps = []
    for b, h in enumerate(heads):
        rows = slice(256 * b, 256 * b + 256)
        rhs = jnp.concatenate([h["v"] * h["beta"], h["kb"] * h["grown"]], axis=1)
        uw = rhs + dot((inv_s[b] - eye).astype(BF16), rhs.astype(BF16))
        uw16 = uw.astype(BF16)
        both = dot(h["scores"], uw16)
        o0[rows, :] = both[:, 0:128]
        pmx[rows, :] = (h["q"] * h["grown"] - both[:, 128:256]).astype(BF16)
        last_run = h["run"][255:256, :]
        kd = (h["k"] * jnp.exp(last_run - h["run"])).astype(BF16)
        ku = dot(kd, uw16, ((0,), (0,)))
        keep = jnp.exp(last_run)
        maps.append((keep, ku[:, 128:256].astype(BF16), ku[:, 0:128]))

    eye128 = (iota((128, 128), 0) == iota((128, 128), 1)).astype(F32)
    keep0, kw0, b0 = maps[0]
    keep1, kw1, b1 = maps[1]
    m0 = eye128 * keep0 - kw0.astype(F32)
    kw0_s[...] = kw0
    b0_s[...] = b0
    keep_s[0:1, :] = keep0
    first_map = jnp.concatenate([m0, b0], axis=1)
    keep1w = jnp.concatenate([keep1, keep1], axis=1)
    core_map = keep1w * first_map - dot(kw1, first_map.astype(BF16))
    core_map = core_map + jnp.concatenate([jnp.zeros_like(b1), b1], axis=1)
    stc[c] = core_map.astype(BF16)
    remote(stc.at[c], stc.at[c], st_ss.at[0], st_rs.at[c], partner)
    arrived(stc.at[1 - c], st_rs.at[1 - c])
    one = stc[1]
    chip_map = dot(one[:, 0:128], stc[0])
    chip_map = chip_map + jnp.concatenate([jnp.zeros_like(b1), one[:, 128:256].astype(F32)], axis=1)
    stz_src[...] = chip_map.astype(BF16)
    for d in (1, 2, 3):
        remote(
            stz_src, stz.at[z], stz_ss.at[d - 1], stz_rs.at[z],
            dev(mod4(z + d), y, x, c), z + d <= 3,
        )

    wo_away_pump((zp, z2), 26)

    @pl.when(first)
    def _():
        pad[0:16, :] = jnp.zeros((16, 128), F32)

    @pl.when(jnp.logical_not(first))
    def _():
        arrived(prev_dst, prev_rs.at[0])
        pad[0:16, :] = ap[256:272, 0:128].astype(F32)

    window = jnp.left_shift(2, y)
    base = 512 * (2 * z + c)
    for b in (0, 1):
        at = 256 * b
        sums = pad[16 + at : 272 + at, :]
        here = sums
        for lag in range(1, 16):
            part = pad[16 + at - lag : 272 + at - lag, :]
            sums = sums + part * jnp.where(lag < window, 1.0, 0.0)
        counts = jnp.minimum(base + at + iota((256, 128), 0) + 1, window).astype(F32)
        pooled = (sums / counts - here).astype(BF16)
        row = packb[b]
        pscale = jnp.where(yodd == 0, row[10:11, 0:128], row[10:11, 128:256])
        pool_src[at : at + 256, :] = (dot(pooled, pmb[...]) * pscale).astype(BF16)

    def spread_out(src, dst, rsem, ssem):
        cols = pl.ds(128 * y, 128)

        @pl.when(home)
        def _():
            dst[0:256, cols] = src[pl.ds(256 * yodd, 256), :]

        for j in (0, 1):
            to_y = 2 * c + j
            here = to_y == y
            rows = pl.ds(256 * j, 256)
            remote(
                src.at[rows, :], dst.at[pl.ds(0, 256), cols], ssem.at[3 * j],
                rsem.at[y], partner, here,
            )
            for r in (0, 1):
                remote(
                    src.at[pl.ds(256 * j + 128 * r, 128), :],
                    dst.at[pl.ds(128 * r, 128), cols],
                    ssem.at[3 * j + 1 + r], rsem.at[y], dev(z, to_y, x, r),
                    jnp.logical_not(here),
                )

    def gather_in(dst, rsem, fsem):
        for i, d in enumerate((1, 3, 2)):
            yy = mod4(me_y + d)
            part = dst.at[pl.ds(128 * c, 128), pl.ds(128 * yy, 128)]
            arrived(part, rsem.at[yy])
            remote(part, part, fsem.at[i], rsem.at[4 + yy], partner)
        for d in (1, 3, 2):
            yy = mod4(me_y + d)
            part = dst.at[pl.ds(128 * (1 - c), 128), pl.ds(128 * yy, 128)]
            arrived(part, rsem.at[4 + yy])

        @pl.when(away)
        def _():
            arrived(dst.at[pl.ds(0, 256), pl.ds(128 * me_y, 128)], rsem.at[me_y])

    spread_out(pool_src, ap, ap_rs, ap_ss)

    state_s[...] = jnp.zeros((128, 128), F32)

    def absorb(part):
        moved = dot(part[:, 0:128], state_s[...].astype(BF16))
        state_s[...] = moved + part[:, 128:256].astype(F32)

    for i in (0, 1, 2):
        @pl.when(i < z)
        def _(i=i):
            arrived(stz.at[i], stz_rs.at[i])
            absorb(stz[i])

    @pl.when(c == 1)
    def _():
        absorb(stc[0])

    hng = pk_v[24:25, 0:128]
    for b in (0, 1):
        rows = slice(256 * b, 256 * b + 256)
        s16 = state_s[...].astype(BF16)
        o = o0[rows, :] + dot(pmx[rows, :], s16)
        gate = silu(acc[rows, 512:640] * row_scale(b))
        norm = lax.rsqrt(jnp.mean(o * o, axis=-1, keepdims=True) + EPS)
        delta_src[rows, :] = (o * norm * hng * gate).astype(BF16)
        if b == 0:
            state_s[...] = keep_s[0:1, :] * state_s[...] - dot(kw0_s[...], s16) + b0_s[...]

    spread_out(delta_src, ad, ad_rs, ad_ss)

    for zz in (z, zm, zp, z2):
        for cc in (0, 1):
            @pl.when(away)
            def _(zz=zz, cc=cc):
                arrived(woslot(zz, yo, cc), wosem(zz, yo, cc))

    gather_in(ap, ap_rs, apf_ss)
    gather_in(ad, ad_rs, adf_ss)

    def piece(zz):
        halves = []
        for j in (0, 1):
            part = None
            for cc in (0, 1):
                cols = slice(256 * cc, 256 * cc + 256)
                term = dot(ap[0:256, cols], wo[zz, 2 * j + cc, 0:256, :])
                term = term + dot(ad[0:256, cols], wo[zz, 2 * j + cc, 256:512, :])
                part = term if part is None else part + term
            halves.append(part)
        return jnp.concatenate(halves, axis=1)

    top, bottom = pl.ds(0, 128), pl.ds(128, 128)
    to_p, to_m = dev(z, y, xp, c), dev(z, y, xm, c)
    rs2[...] = piece(x2).astype(BF16)
    remote(rs2.at[top, :], rl.at[0], rs_ss.at[0], rs_rs.at[0], to_p)
    remote(rs2.at[bottom, :], rl.at[1], rs_ss.at[1], rs_rs.at[1], to_m)
    up_s[...] = piece(xp)
    rsp[128:256, :] = up_s[128:256, :].astype(BF16)
    remote(rsp.at[bottom, :], rin.at[0, bottom, :], rs_ss.at[2], rs_rs.at[2], to_p)
    down_s[...] = piece(xm)
    rsm[0:128, :] = down_s[0:128, :].astype(BF16)
    remote(rsm.at[top, :], rin.at[1, top, :], rs_ss.at[3], rs_rs.at[3], to_m)
    arrived(rl.at[0], rs_rs.at[0])
    rsp[0:128, :] = (up_s[0:128, :] + rl[0].astype(F32)).astype(BF16)
    remote(rsp.at[top, :], rin.at[0, top, :], rs_ss.at[4], rs_rs.at[4], to_p)
    arrived(rl.at[1], rs_rs.at[1])
    rsm[128:256, :] = (down_s[128:256, :] + rl[1].astype(F32)).astype(BF16)
    remote(rsm.at[bottom, :], rin.at[1, bottom, :], rs_ss.at[5], rs_rs.at[5], to_m)
    mine = piece(x)
    arrived(rin.at[0, bottom, :], rs_rs.at[2])
    arrived(rin.at[1, top, :], rs_rs.at[3])
    arrived(rin.at[0, top, :], rs_rs.at[4])
    arrived(rin.at[1, bottom, :], rs_rs.at[5])
    out_ref[...] = (mine + rin[0].astype(F32) + rin[1].astype(F32)).astype(BF16)

    for end in ends:
        end()


def per_device(
    inputs, input_norm_gain, pooling_input_weight, query_weight, key_weight,
    value_weight, gate_weight, decay_weight, strength_weight, pooling_group_map,
    pooling_scale, head_log_decay, decay_logit_bias, write_logit_bias,
    decay_position_factor, decay_position_offset, head_norm_gain,
    pooling_output_weight, delta_output_weight,
):
    def wide(rows):
        rows = rows.astype(F32)
        return jnp.pad(rows, ((0, 0), (0, 512 - rows.shape[1])))

    def level(a):
        return wide(jnp.broadcast_to(a[:, None], (2, 256)))

    table = jnp.concatenate(
        [
            input_norm_gain.astype(F32).reshape(8, 512),
            wide(decay_position_factor.T),
            wide(decay_position_offset.T),
            level(head_log_decay),
            level(decay_logit_bias),
            level(write_logit_bias),
            wide(pooling_scale[None]),
            jnp.zeros((5, 512), F32),
            wide(head_norm_gain[None]),
            jnp.zeros((7, 512), F32),
        ],
        axis=0,
    )
    dma = pltpu.SemaphoreType.DMA
    vmem = pltpu.VMEM
    hbm = pl.BlockSpec(memory_space=pl.ANY)
    local = pl.BlockSpec(memory_space=pltpu.VMEM)
    return pl.pallas_call(
        kernel,
        out_shape=jax.ShapeDtypeStruct((256, 512), BF16),
        in_specs=[hbm] * 10 + [local] * 3,
        out_specs=local,
        scratch_shapes=[
            vmem((8, 512, 512), BF16),
            vmem((32, 128, 768), BF16),
            vmem((4, 4, 512, 256), BF16),
            vmem((2, 16, 512), F32),
            vmem((128, 128), BF16),
            vmem((512, 512), BF16),
            vmem((512, 768), F32),
            vmem((512, 128), F32),
            vmem((2, 128, 256), BF16),
            vmem((128, 256), BF16),
            vmem((4, 128, 256), BF16),
            vmem((528, 128), F32),
            vmem((512, 128), BF16),
            vmem((512, 128), BF16),
            vmem((16, 128), BF16),
            vmem((272, 512), BF16),
            vmem((256, 512), BF16),
            vmem((256, 512), BF16),
            vmem((256, 512), BF16),
            vmem((256, 512), BF16),
            vmem((2, 128, 512), BF16),
            vmem((2, 256, 512), BF16),
            vmem((512, 128), F32),
            vmem((512, 128), BF16),
            vmem((128, 128), BF16),
            vmem((128, 128), F32),
            vmem((8, 128), F32),
            vmem((2, 256, 256), F32),
            vmem((2, 256, 256), F32),
            vmem((256, 512), F32),
            vmem((256, 512), F32),
            vmem((128, 128), F32),
            dma((16,)), dma((32,)), dma((16,)), dma((2,)), dma((1,)), dma((2,)),
            dma((4,)), dma((1,)), dma((8,)), dma((8,)), dma((6,)),
            dma((5,)), dma((13,)), dma((20,)), dma((32,)), dma((6,)), dma((28,)),
            dma((2,)), dma((1,)), dma((1,)), dma((3,)), dma((1,)),
            dma((6,)), dma((6,)), dma((3,)), dma((3,)), dma((6,)),
        ],
        compiler_params=pltpu.CompilerParams(
            collective_id=0, has_side_effects=True, vmem_limit_bytes=60 * 1024 * 1024
        ),
    )(
        inputs, pooling_input_weight, query_weight, key_weight, value_weight,
        gate_weight, pooling_output_weight, delta_output_weight, table,
        pooling_group_map, table, decay_weight, strength_weight,
    )


def solution(mesh):
    rows, heads = P("sp", "tp"), P("tp")
    in_specs = (
        rows, P(), rows, rows, rows, rows, rows, P(), P(), P("tp", None, None),
        heads, heads, heads, heads, rows, rows, P(), P("tp", "sp"), P("tp", "sp"),
    )
    return jax.shard_map(
        per_device, mesh=mesh, in_specs=in_specs, out_specs=rows, check_vma=False
    )
```

time: 292 us -> 100 us (0.34); the launches traced: 288 us -> 99.8 us
  waiting for transfers between devices: 101 us -> 0 us
  Pallas kernels: 0 us -> 87.3 us
  other arithmetic: 53.7 us -> 0 us
  matrix products: 41.6 us -> 0 us
  blocking collectives: 39 us -> 0 us
  local copies, waits for them, and re-layouts: 29 us -> 12.5 us
  between operations: 13.9 us -> 0.04 us
  starting transfers between devices: 9.67 us -> 0 us
    pallas_call x0 -> x1, Pallas kernels: none -> 87.3 us  [per_device(): pl.pallas_call(kernel, out_shape=jax.ShapeDtypeStruct((256, 512), BF16),...]
    all_gather x2 -> x0, waiting for transfers between devices: 42.9 us -> none  [the longest x1 42.9 us: in_one_piece(): out = lax.all_gather(both, axis, axis=dim, tiled=True)]
    reduce_scatter x1 -> x0, waiting for transfers between devices: 40.9 us -> none  [per_device(): lax.psum_scatter(partial_value.astype(jnp.bfloat16), 'tp', scatter_dimens...]
    another operation x4 -> x0, other arithmetic: 40.4 us -> none  [the longest x2 39.9 us: block_terms(): jax.scipy.linalg.solve_triangular(system, value_matrix * write_strength_r...]
    all_gather x4 -> x0, blocking collectives: 39 us -> none  [carried_in(): lax.all_gather(part.astype(kind), axis)]
    dot_general x49 -> x0, matrix products: 38.4 us -> none  [the longest x5 13.3 us: per_device(): jnp.dot(normed, weight_piece, preferred_element_type=jnp.float32)]
    all_to_all x1 -> x0, waiting for transfers between devices: 17 us -> none  [from_everyone(): lax.all_to_all(jnp.broadcast_to(shard[None], (peers, *shard.shape)), axis...]
    convert_element_type x15 -> x0, other arithmetic: 8.83 us -> none  [the longest x8 4.78 us: pool_branch(): (lag_index < windows).astype(jnp.float32)[None, :, None]]
  transfers between devices with their start and end apart: 5 -> 0, of which waited for: 3 -> 0; matrix products, arithmetic and copies ran while one was open for 39% -> 0% of each run, Pallas kernels for 0% -> 0%
where the time goes in v1:
time: 100 us; the launch traced here: 99.8 us
  Pallas kernels  87.3 us (87%)
  local copies, waits for them, and re-layouts  12.5 us (12%)
    pallas_call x1, Pallas kernels, per_device(): pl.pallas_call(kernel, out_shape=jax.ShapeDtypeStruct((256, 512), BF16),...  87.3 us
    unnamed x7, local copies, waits for them, and re-layouts  4.37 us
    pad x7, local copies, waits for them, and re-layouts, wide(): return jnp.pad(rows, ((0, 0), (0, 512 - rows.shape[1])))  2.77 us
    concatenate x1, local copies, waits for them, and re-layouts, per_device(): jnp.concatenate([input_norm_gain.astype(F32).reshape(8, 512), wide(decay_...  2.47 us
    broadcast_in_dim x3, local copies, waits for them, and re-layouts, level(): return wide(jnp.broadcast_to(a[:, None], (2, 256)))  2.17 us

profile of v1, /device:TPU:1, one launch (start us, length us, event | category | flops | bytes accessed | tf_op | source)
XLA Modules:
  0.0 99.8 jit_solution(7178366158734757353)
XLA Ops:
  0.0 0.0 copy-start
  0.0 0.7 pad.29
  0.7 0.7 broadcast_in_dim.14
  1.5 0.7 broadcast_in_dim.15
  2.2 0.7 broadcast_in_dim.32
  2.9 0.7 pad.30
  3.6 0.7 pad.24
  4.3 0.7 pad.25
  4.9 0.7 reshape.12
  5.7 2.5 %concatenate.3.pk_in.pk_v = f32[32,512]{1,0:T(8,128)} concatenate(f32[8,512]{1,0:T(8,128)S(1)} %reshape.12, f32[2,512]{1,0:T(2,128)S(1)} %pad.24, f32[2,512]{1,0:T(2,128)S(1)} %pad.25, f32[2,512]{1,0:T(2,128)S(1)} %pad.26, f32[2,512]{1,0:T(2,128)S(1)} %pad.27, f32[2,512]{1,0:T(2,128)S(1)} %pad.28, f32[1,512]{1,0:T(1,128)S(1)} %pad.29, f32[5,512]{1,0:T(8,128)S(1)} %broadcast_in_dim.34, ...), dimensions={0} | concatenate | bytes 131072 | tf_op jit(solution)/shard_map/concatenate | solution.py:574
  8.2 0.0 copy-done
  8.2 0.0 copy-start.1
  8.2 1.3 %copy.20.dw_v = bf16[4096,16]{1,0:T(8,128)(2,1)} copy(bf16[4096,16]{0,1:T(8,128)(2,1)S(1)} %copy-done) | data formatting | bytes 262144 | tf_op args[7]
  9.5 0.0 copy-done.1
  9.5 1.4 %copy.21.sw_v = bf16[4096,16]{1,0:T(8,128)(2,1)} copy(bf16[4096,16]{0,1:T(8,128)(2,1)S(1)} %copy-done.1) | data formatting | bytes 262144 | tf_op args[8]
  10.9 87.3 %shard_map.181 = bf16[256,512]{1,0:T(8,128)(2,1)} custom-call(bf16[256,512]{1,0:T(8,128)(2,1)} %x_in.1, bf16[256,256]{1,0:T(8,128)(2,1)} %wp_in.1, bf16[256,256]{1,0:T(8,128)(2,1)} %wq_in.1, bf16[256,256]{1,0:T(8,128)(2,1)} %wk_in.1, bf16[256,256]{1,0:T(8,128)(2,1)} %wv_in.1, bf16[256,256]{1,0:T(8,128)(2,1)} %wg_in.1, bf16[256,256]{1,0:T(8,128)(2,1)} %op_in.1, ...), custom_call_target="tpu_custom_call" | custom-call | tf_op jit(solution)/shard_map/pallas_call | solution.py:593
  98.2 1.7 %copy.23 = bf16[256,512]{1,0:T(8,128)(2,1)} copy(bf16[256,512]{1,0:T(8,128)(2,1)} %shard_map.181) | data formatting | bytes 524288
  (5 shorter events, 0.0 us)
Async XLA Ops:
  0.0 8.2 %copy-start = (bf16[4096,16]{0,1:T(8,128)(2,1)S(1)}, bf16[4096,16]{0,1:T(8,128)(2,1)}, u32[]{:S(2)}) copy-start(bf16[4096,16]{0,1:T(8,128)(2,1)} %param.26) | copy-start | bytes 393220
  8.2 1.3 %copy-start.1 = (bf16[4096,16]{0,1:T(8,128)(2,1)S(1)}, bf16[4096,16]{0,1:T(8,128)(2,1)}, u32[]{:S(2)}) copy-start(bf16[4096,16]{0,1:T(8,128)(2,1)} %param.27) | copy-start | bytes 393220

commit v2 on v1

--- a/solution.py
+++ b/solution.py
@@ -34,13 +34,14 @@
 
 
 def kernel(
-    x_in, wp_in, wq_in, wk_in, wv_in, wg_in, op_in, od_in, pk_in, pm_in,
-    pk_v, dw_v, sw_v,
+    x_in, wp_in, wq_in, wk_in, wv_in, wg_in, op_in, od_in, pm_in,
+    hld_in, dlb_in, wlb_in, gain_in, factor_in, offset_in, pscale_in, hng_in, dw_in, sw_in,
     out_ref,
-    xbuf, wbuf, wo, packb, pmb, xg, acc, ssq,
-    stc, stz_src, stz, pad, pool_src, delta_src, prev_src, ap, ad,
+    hld_v, dlb_v, wlb_v, gain_v, factor_v, offset_v, pscale_v, hng_v, rates_v,
+    xbuf, wbuf, wo, gain_f, pk_src, packb, pmb, xg, acc, ssq,
+    w_stage, stc, stz_src, stz, pad, pool_src, delta_src, prev_src, ap, ad,
     rs2, rsp, rsm, rl, rin, o0, pmx, kw0_s, b0_s, keep_s, low_s, inv_s, up_s, down_s, state_s,
-    x_rs, w_rs, wo_rs, pk_rs, pm_rs, st_rs, stz_rs, prev_rs, ap_rs, ad_rs, rs_rs,
+    in_rs, ws_rs, x_rs, w_rs, wo_rs, pk_rs, pm_rs, st_rs, stz_rs, prev_rs, ap_rs, ad_rs, rs_rs,
     x_ss, xf_ss, w_ss, wf_ss, wo_ss, wof_ss, pk_ss, pm_ss, st_ss, stz_ss, prev_ss,
     ap_ss, ad_ss, apf_ss, adf_ss, rs_ss,
 ):
@@ -91,6 +92,14 @@
     def arrived(ref, sem):
         pltpu.make_async_copy(ref, ref, sem).wait()
 
+    loads = [
+        (hld_in, hld_v), (dlb_in, dlb_v), (wlb_in, wlb_v), (factor_in, factor_v),
+        (offset_in, offset_v), (pscale_in, pscale_v), (gain_in, gain_v), (hng_in, hng_v),
+        (dw_in, rates_v.at[pl.ds(0, 16), :]), (sw_in, rates_v.at[pl.ds(16, 16), :]),
+    ]
+    for i, (src, dst) in enumerate(loads):
+        pltpu.make_async_copy(src, dst, in_rs.at[i]).start()
+
     barrier = pltpu.get_barrier_semaphore()
     peers = [partner]
     for d in (1, 2, 3):
@@ -102,11 +111,14 @@
         pl.semaphore_signal(barrier, inc=1, device_id=to, device_id_type=MESH)
     pl.semaphore_wait(barrier, len(peers))
 
-    def xslot(yy, xx, cc):
-        return xbuf.at[2 * xx + cc, pl.ds(256 * lax.rem(yy, 2), 256), :]
-
-    def xsem(yy, xx, cc):
-        return x_rs.at[8 * lax.rem(yy, 2) + 2 * xx + cc]
+    def xslot(yy, xx, u, quarter=None):
+        start, size = 128 * (u % 2), 128
+        if quarter is not None:
+            start, size = start + 64 * quarter, 64
+        return xbuf.at[2 * xx + u // 2, pl.ds(256 * lax.rem(yy, 2) + start, size), :]
+
+    def xsem(yy, xx, u):
+        return x_rs.at[16 * lax.rem(yy, 2) + 4 * xx + u]
 
     def wslot(zz, yy, r):
         return wbuf.at[2 * (4 * zz + yy) + r, :, pl.ds(0, 640)]
@@ -114,83 +126,109 @@
     def wsem(zz, yy, r):
         return w_rs.at[2 * (4 * zz + yy) + r]
 
-    def woslot(zz, yy, cc):
-        return wo.at[zz, 2 * lax.rem(yy, 2) + cc]
+    def woslot(zz, yy, cc, half=None):
+        block = wo.at[zz, 2 * lax.rem(yy, 2) + cc]
+        return block if half is None else block.at[pl.ds(256 * half, 256), :]
 
     def wosem(zz, yy, cc):
         return wo_rs.at[4 * zz + 2 * lax.rem(yy, 2) + cc]
 
-    own = xslot(y, x, c)
-    own_sem = xsem(y, x, c)
-    remote(x_in, own, x_ss.at[0], own_sem, dev(z, y, xp, kh))
-    remote(x_in, own, x_ss.at[1], own_sem, dev(z, y, xm, kh))
-    remote(x_in, own, x_ss.at[2], own_sem, dev(z, yp, x, kh))
-    remote(x_in, own, x_ss.at[3], own_sem, dev(z, ym, x, kh))
-    remote(x_in, own, x_ss.at[4], own_sem, partner, away)
-
-    @pl.when(home)
-    def _():
-        pltpu.make_async_copy(x_in, own, own_sem).start()
-
-    wo_own = woslot(z, y, c)
-    for half, ref in enumerate((op_in, od_in)):
-        part = wo_own.at[pl.ds(256 * half, 256), :]
-        for i, zz in enumerate((zp, zm)):
-            remote(ref, part, wo_ss.at[2 * half + i], wosem(z, y, c), dev(zz, y, x, kh))
-        remote(ref, part, wo_ss.at[4 + half], wosem(z, y, c), partner, away)
+    def own_x(half):
+        src = x_in.at[pl.ds(128 * half, 128), :]
+        dst = xbuf.at[tp, pl.ds(256 * yodd + 128 * half, 128), :]
+        return src, dst, x_rs.at[16 * yodd + 2 * tp + half]
+
+    def own_x_along_y(half, cond=None):
+        src, dst, sem = own_x(half)
+        for i, yy in enumerate((yp, ym)):
+            at = 6 + 2 * half + i
+            remote(src, dst, x_ss.at[at], sem, dev(z, yy, x, kh), cond)
+
+    for half in (1, 0):
+        src, dst, sem = own_x(half)
+        for i, xx in enumerate((xp, xm)):
+            remote(src, dst, x_ss.at[3 * half + i], sem, dev(z, y, xx, kh))
+        remote(src, dst, x_ss.at[3 * half + 2], sem, partner, away)
 
         @pl.when(home)
-        def _(ref=ref, part=part):
-            pltpu.make_async_copy(ref, part, wosem(z, y, c)).start()
+        def _(src=src, dst=dst, sem=sem):
+            pltpu.make_async_copy(src, dst, sem).start()
+
+    own_x_along_y(0)
+    own_x_along_y(1, c == 0)
+
+    def both(p, q):
+        return jnp.logical_and(p, q)
 
     for j in (0, 1):
+        same = yodd == j
+        for r in (0, 1):
+            far = dev(z, yp if r == 0 else ym, x, r)
+            for n, ref in enumerate((wp_in, wq_in, wk_in, wv_in, wg_in)):
+                src = ref.at[pl.ds(128 * r, 128), pl.ds(128 * j, 128)]
+                dst = w_stage.at[:, pl.ds(128 * n, 128)]
+                remote(src, dst, w_ss.at[10 * j + 5 * r + n], ws_rs.at[0], far, both(away, same))
+    for j in (0, 1):
+        same = yodd == j
         head_y = 2 * c + j
         for r in (0, 1):
-            self_here = jnp.logical_and(head_y == y, c == r)
+            here = both(both(home, same), c == r)
+            direct = jnp.logical_not(jnp.logical_or(here, both(away, same)))
             for n, ref in enumerate((wp_in, wq_in, wk_in, wv_in, wg_in)):
                 src = ref.at[pl.ds(128 * r, 128), pl.ds(128 * j, 128)]
                 dst = wbuf.at[2 * sp + r, :, pl.ds(128 * n, 128)]
                 remote(
-                    src, dst, w_ss.at[5 * (2 * j + r) + n], wsem(z, y, r),
-                    dev(z, head_y, x, r), jnp.logical_not(self_here),
+                    src, dst, w_ss.at[20 + 10 * j + 5 * r + n], wsem(z, y, r),
+                    dev(z, head_y, x, r), direct,
                 )
 
-                @pl.when(self_here)
+                @pl.when(here)
                 def _(src=src, dst=dst, r=r):
                     pltpu.make_async_copy(src, dst, wsem(z, y, r)).start()
 
+    wo_own = wo.at[z, 2 * yodd + c]
+    own_sem = wo_rs.at[4 * z + 2 * yodd + c]
+
+    def own_wo(tos, at):
+        for half, ref in enumerate((op_in, od_in)):
+            part = wo_own.at[pl.ds(256 * half, 256), :]
+            for i, to in enumerate(tos):
+                remote(ref, part, wo_ss.at[at + 2 * half + i], own_sem, to)
+
+    own_wo((dev(zp, y, x, kh), dev(zm, y, x, kh)), 0)
+    for half, ref in enumerate((op_in, od_in)):
+        part = wo_own.at[pl.ds(256 * half, 256), :]
+        remote(ref, part, wo_ss.at[8 + half], own_sem, partner, away)
+
+        @pl.when(home)
+        def _(ref=ref, part=part):
+            pltpu.make_async_copy(ref, part, own_sem).start()
+
+    for i, (src, dst) in enumerate(loads):
+        pltpu.make_async_copy(src, dst, in_rs.at[i]).wait()
+    pk_src[0:2, :] = factor_v[...]
+    pk_src[2:4, :] = offset_v[...]
+    for j in (0, 1):
+        for at, ref in ((4, hld_v), (6, dlb_v), (8, wlb_v)):
+            pk_src[at + j : at + j + 1, :] = jnp.broadcast_to(ref[0:1, j : j + 1], (1, 256))
+    pk_src[10:11, :] = pscale_v[...]
     for j in (0, 1):
         head_y = 2 * c + j
         self_here = jnp.logical_and(head_y == y, home)
-        src = pk_in.at[pl.ds(8, 16), :]
-        dst = packb.at[yodd]
         remote(
-            src, dst, pk_ss.at[j], pk_rs.at[yodd], dev(z, head_y, x, kh),
+            pk_src, packb.at[yodd], pk_ss.at[j], pk_rs.at[yodd], dev(z, head_y, x, kh),
             jnp.logical_not(self_here),
         )
 
         @pl.when(self_here)
-        def _(src=src, dst=dst):
-            pltpu.make_async_copy(src, dst, pk_rs.at[yodd]).start()
+        def _():
+            packb[yodd] = pk_src[...]
 
     remote(pm_in.at[yodd], pmb, pm_ss.at[0], pm_rs.at[0], partner, home)
 
     @pl.when(home)
     def _():
         pltpu.make_async_copy(pm_in.at[yodd], pmb, pm_rs.at[0]).start()
-
-    head = 4 * x + y
-    row16, col16 = iota((16, 128), 0), iota((16, 128), 1)
-    pick_d = jnp.logical_and(row16 == head, col16 == 0).astype(BF16)
-    pick_s = jnp.logical_and(row16 == head, col16 == 1).astype(BF16)
-
-    def fill(i, carry):
-        rows = pl.ds(pl.multiple_of(128 * i, 128), 128)
-        both = dot(dw_v[rows, :], pick_d) + dot(sw_v[rows, :], pick_s)
-        wbuf[i, :, 640:768] = both.astype(BF16)
-        return carry
-
-    lax.fori_loop(0, 32, fill, 0)
 
     def w_first(d, n):
         yy = mod4(me_y + d)
@@ -211,82 +249,63 @@
     yn = 2 * c + 1 - yodd
     yo = 2 * c + yodd
     from_below = mod4(yn + 1) == y
-    relay_c = jnp.where(from_below, 0, 1)
+    relay_half = jnp.where(from_below, 0, 1)
     y_next = jnp.where(from_below, yp, ym)
-
-    w_first(0, 0)
-    for cc in (0, 1):
-        slot = xslot(yn, x, cc)
-        arrived(slot, xsem(yn, x, cc))
-        remote(slot, slot, xf_ss.at[2 * cc], xsem(yn, x, cc), dev(z, y, xp, c))
-        remote(slot, slot, xf_ss.at[2 * cc + 1], xsem(yn, x, cc), dev(z, y, xm, c))
-    slot = xslot(yn, x, relay_c)
-    remote(slot, slot, xf_ss.at[4], xsem(yn, x, relay_c), dev(z, y_next, x, c))
-    w_first(1, 3)
-    w_first(3, 6)
-    for cc in (0, 1):
-        slot = xslot(yo, x, cc)
-        arrived(slot, xsem(yo, x, cc))
-        remote(slot, slot, xf_ss.at[5 + 2 * cc], xsem(yo, x, cc), dev(z, y, xp, c), away)
-        remote(slot, slot, xf_ss.at[6 + 2 * cc], xsem(yo, x, cc), dev(z, y, xm, c), away)
-    w_first(2, 9)
+    xf_n = iter(range(64))
+    wof_n = iter(range(64))
+
+    def wait_if(cond, slot, sem):
+        if cond is None:
+            arrived(slot, sem)
+        else:
+            @pl.when(cond)
+            def _():
+                arrived(slot, sem)
+
+    def x_pass(yy, xx, u, tos, relay=None, cond=None):
+        slot, sem = xslot(yy, xx, u), xsem(yy, xx, u)
+        wait_if(cond, slot, sem)
+        for to in tos:
+            remote(slot, slot, xf_ss.at[next(xf_n)], sem, to, cond)
+        if relay is not None:
+            half, to = relay
+            part = xslot(yy, xx, u, half)
+            remote(part, part, xf_ss.at[next(xf_n)], sem, to, cond)
+
+    def wo_pass(zz, yy, cc, tos, relay=None, cond=None):
+        slot, sem = woslot(zz, yy, cc), wosem(zz, yy, cc)
+        wait_if(cond, slot, sem)
+        for to in tos:
+            remote(slot, slot, wof_ss.at[next(wof_n)], sem, to, cond)
+        if relay is not None:
+            half, to = relay
+            part = woslot(zz, yy, cc, half)
+            remote(part, part, wof_ss.at[next(wof_n)], sem, to, cond)
+
+    FIRST_Y, FIRST_X = (0, 1, 2), (3,)
+    x_ring = (dev(z, y, xp, c), dev(z, y, xm, c))
+    y_ring = (dev(z, yp, x, c), dev(z, ym, x, c))
+    z_ring = (dev(zp, y, x, c), dev(zm, y, x, c))
+    y_relay = (relay_half, dev(z, y_next, x, c))
 
     yf = jnp.where(home, yo, yn)
     yl = jnp.where(home, yn, yo)
-    n = 9
-    for yy in (yf, yl):
-        for xx, cc, to_x in ((xm, 0, xp), (xp, 1, xm)):
-            slot = xslot(yy, xx, cc)
-            arrived(slot, xsem(yy, xx, cc))
-            remote(slot, slot, xf_ss.at[n], xsem(yy, xx, cc), dev(z, y, to_x, c))
-            n += 1
-
-    def wo_home(zz, cc, n, to_z=None):
-        @pl.when(home)
-        def _():
-            slot = woslot(zz, me_y, cc)
-            arrived(slot, wosem(zz, me_y, cc))
-
-        slot = woslot(zz, me_y, cc)
-        sem = wosem(zz, me_y, cc)
-        if to_z is not None:
-            remote(slot, slot, wof_ss.at[n], sem, dev(to_z, y, x, c), home)
-        remote(slot, slot, wof_ss.at[n + 1], sem, dev(z, yp, x, c), home)
-        remote(slot, slot, wof_ss.at[n + 2], sem, dev(z, ym, x, c), home)
-
-    wo_home(z, 0, 0)
-    wo_home(z, 1, 3)
-    wo_home(zm, 0, 6, zp)
-    wo_home(zp, 1, 9, zm)
-
-    n = 12
-    for d in (0, 1, 3, 2):
-        w_later(zm, d, n, zp if d in (0, 2) else None)
-        w_later(zp, d, n + 2, zm if d in (1, 3) else None)
-        n += 4
-
-    wo_home(zm, 1, 12)
-    wo_home(zp, 0, 15)
-    wo_home(z2, 0, 18)
-    wo_home(z2, 1, 21)
-
-    for d in (0, 1, 3, 2):
-        w_later(z2, d, n)
-        n += 1
-
-    for yy in (yn, yo):
-        for xx, cc in ((xm, 1), (xp, 0), (x2, 0), (x2, 1)):
-            arrived(xslot(yy, xx, cc), xsem(yy, xx, cc))
-    for zz in (z, zp, zm, z2):
-        for d in (0, 1, 2, 3):
-            yy = mod4(y + d)
-            arrived(wslot(zz, yy, 1 - c), wsem(zz, yy, 1 - c))
-
-    ssq[...] = jnp.zeros_like(ssq)
-    acc[...] = jnp.zeros_like(acc)
-
-    def project(i, carry):
-        gain = pk_v[pl.ds(i, 1), :]
+
+    def fill(i, carry):
+        rows = pl.ds(pl.multiple_of(512 * i, 512), 512)
+        both_cols = dot(rates_v[:, rows], pick, ((0,), (0,))).astype(BF16)
+        wbuf[pl.ds(4 * i, 4), :, 640:768] = both_cols.reshape(4, 128, 128)
+        return carry
+
+    head = 4 * x + y
+    row32, col32 = iota((32, 128), 0), iota((32, 128), 1)
+    pick = jnp.logical_or(
+        jnp.logical_and(row32 == head, col32 == 0),
+        jnp.logical_and(row32 == head + 16, col32 == 1),
+    ).astype(BF16)
+
+    def project(i):
+        gain = gain_f[pl.ds(i, 1), :]
         for b in range(4):
             rows = slice(128 * b, 128 * b + 128)
             v = xbuf[i, rows, :].astype(F32)
@@ -296,22 +315,97 @@
             )
             xg[rows, :] = (v * gain).astype(BF16)
         acc[...] += dot(xg[...], wbuf[pl.ds(4 * i, 4)].reshape(512, 768))
-        return carry
-
-    lax.fori_loop(0, 8, project, 0)
-
-    def wo_away_pump(zs, n):
-        for zz in zs:
-            for cc in (0, 1):
-                arrived(woslot(zz, yn, cc), wosem(zz, yn, cc))
-            slot = woslot(zz, yn, relay_c)
-            remote(slot, slot, wof_ss.at[n], wosem(zz, yn, relay_c), dev(z, y_next, x, c))
-            n += 1
-
-    wo_away_pump((z, zm), 24)
+
+    w_first(0, 0)
+    for u in FIRST_X:
+        x_pass(y, xm, u, y_ring, (0, x_ring[0]), home)
+        x_pass(y, xp, u, y_ring, (1, x_ring[1]), home)
+    for u in FIRST_Y:
+        x_pass(yn, x, u, x_ring, y_relay)
+    arrived(w_stage, ws_rs.at[0])
+    stage_from = jnp.where(c == 0, ym, yp)
+    stage_to = jnp.where(c == 0, yp, ym)
+    stage_dst = wbuf.at[2 * (4 * z + stage_from) + c, :, pl.ds(0, 640)]
+    remote(w_stage, stage_dst, w_ss.at[40], wsem(z, stage_from, c), dev(z, stage_to, x, c))
+    for u in FIRST_Y:
+        x_pass(y, xm, u, (), (0, x_ring[0]), home)
+        x_pass(y, xp, u, (), (1, x_ring[1]), home)
+    w_first(1, 3)
+    w_first(3, 6)
+    own_x_along_y(1, c == 1)
+    for u in FIRST_Y:
+        x_pass(yo, x, u, x_ring, None, away)
+    for u in FIRST_Y:
+        x_pass(yn, xm, u, (), (0, x_ring[0]))
+        x_pass(yn, xp, u, (), (1, x_ring[1]))
+    for u in FIRST_X:
+        x_pass(yn, x, u, (), y_relay)
+    lax.fori_loop(0, 8, fill, 0)
+    gain_f[...] = gain_v[...].astype(F32)
+    ssq[...] = jnp.zeros_like(ssq)
+    acc[...] = jnp.zeros_like(acc)
+    w_first(2, 9)
+    own_wo((dev(z, yp, x, kh), dev(z, ym, x, kh)), 4)
+    for u in FIRST_X:
+        x_pass(y, x2, u, y_ring, None, home)
+        x_pass(yn, xm, u, (), y_relay)
+        x_pass(yn, xp, u, (), y_relay)
+    n = 12
+    for d in (0, 1):
+        w_later(zm, d, n, zp if d in (0, 2) else None)
+        w_later(zp, d, n + 2, zm if d in (1, 3) else None)
+        n += 4
+    for u in FIRST_Y:
+        x_pass(yo, xm, u, (), (0, x_ring[0]), away)
+        x_pass(yo, xp, u, (), (1, x_ring[1]), away)
+    wo_pass(zm, y, 0, y_ring, (0, z_ring[0]), home)
+    wo_pass(zp, y, 0, y_ring, (1, z_ring[1]), home)
+    for d in (3, 2):
+        w_later(zm, d, n, zp if d in (0, 2) else None)
+        w_later(zp, d, n + 2, zm if d in (1, 3) else None)
+        n += 4
+    for u in FIRST_X:
+        x_pass(yn, x2, u, (), y_relay)
+
+    for u in FIRST_X:
+        wait_if(home, xslot(y, x, u), xsem(y, x, u))
+        for xx in (x, xm, xp):
+            wait_if(away, xslot(yo, xx, u), xsem(yo, xx, u))
+    for u in FIRST_Y:
+        wait_if(home, xslot(y, x, u), xsem(y, x, u))
+    for zz in (z, zp, zm):
+        for d in (0, 1, 2, 3):
+            yy = mod4(y + d)
+            arrived(wslot(zz, yy, 1 - c), wsem(zz, yy, 1 - c))
+    gap = mod4(x - z)
+    e0 = jnp.where(gap == 2, xp, x)
+    e1 = jnp.where(gap == 2, xm, jnp.where(gap == 0, xp, z))
+    for i in (e0, e1):
+        lax.fori_loop(2 * i, 2 * i + 2, lambda k, carry: (project(k), carry)[1], 0)
+
+    wo_pass(z, yn, 1, z_ring, y_relay)
+    for d in (0, 1, 3, 2):
+        w_later(z2, d, n)
+        n += 1
+
+    for yy in (yn, yo):
+        for u in FIRST_Y:
+            arrived(xslot(yy, x2, u), xsem(yy, x2, u))
+    for u in FIRST_X:
+        wait_if(away, xslot(yo, x2, u), xsem(yo, x2, u))
+    for d in (0, 1, 2, 3):
+        yy = mod4(y + d)
+        arrived(wslot(z2, yy, 1 - c), wsem(z2, yy, 1 - c))
+    l0 = jnp.where(gap == 2, x, jnp.where(gap == 0, xm, x2))
+    l1 = jnp.where(gap == 2, z, jnp.where(gap == 0, x2, mod4(z + 2)))
+
+    for i in (l0, l1):
+        lax.fori_loop(2 * i, 2 * i + 2, lambda k, carry: (project(k), carry)[1], 0)
 
     for b in (0, 1):
-        arrived(packb.at[b], pk_rs.at[b])
+        @pl.when(jnp.logical_or(away, yodd != b))
+        def _(b=b):
+            arrived(packb.at[b], pk_rs.at[b])
     arrived(pmb, pm_rs.at[0])
 
     ii, jj = iota((256, 256), 0), iota((256, 256), 1)
@@ -345,8 +439,8 @@
         v = silu(acc[rows, 384:512] * s)
         rate = acc[rows, 640:768] * s
         table = packb[b]
-        pick = lambda r: jnp.where(yodd == 0, table[r : r + 1, 0:256], table[r + 1 : r + 2, 0:256])
-        factor, offset, hld, dlb, wlb = (pick(r) for r in (0, 2, 4, 6, 8))
+        of = lambda r: jnp.where(yodd == 0, table[r : r + 1, :], table[r + 1 : r + 2, :])
+        factor, offset, hld, dlb, wlb = (of(r) for r in (0, 2, 4, 6, 8))
         pre = rate.T[0:1, :] + dlb
         soft = jnp.maximum(pre, 0.0) + jnp.log1p(jnp.exp(-jnp.abs(pre)))
         log_decay = -jnp.exp(hld) * soft * factor + offset
@@ -365,6 +459,9 @@
         inv_s[b] = inverse
         heads.append(dict(q=q, k=k, v=v, scores=scores, run=run, grown=grown, kb=kb, beta=beta))
 
+    wo_pass(z, yo, 1, z_ring, None, away)
+    wo_pass(z2, y, 0, y_ring, None, home)
+    wo_pass(z, yn, 0, (), y_relay)
     for level in range(1, 8):
         mask = jnp.right_shift(diff, level) == 1
         mids = []
@@ -413,7 +510,11 @@
             dev(mod4(z + d), y, x, c), z + d <= 3,
         )
 
-    wo_away_pump((zp, z2), 26)
+    for yy in (yf, yl):
+        wo_pass(zm, yy, 1, (), (0, z_ring[0]))
+        wo_pass(zp, yy, 1, (), (1, z_ring[1]))
+    for zz in (zm, zp):
+        wo_pass(zz, yn, 0, (), y_relay)
 
     @pl.when(first)
     def _():
@@ -495,7 +596,7 @@
     def _():
         absorb(stc[0])
 
-    hng = pk_v[24:25, 0:128]
+    hng = hng_v[...]
     for b in (0, 1):
         rows = slice(256 * b, 256 * b + 256)
         s16 = state_s[...].astype(BF16)
@@ -508,11 +609,13 @@
 
     spread_out(delta_src, ad, ad_rs, ad_ss)
 
+    wo_pass(z2, yn, 0, (), y_relay)
     for zz in (z, zm, zp, z2):
-        for cc in (0, 1):
-            @pl.when(away)
-            def _(zz=zz, cc=cc):
-                arrived(woslot(zz, yo, cc), wosem(zz, yo, cc))
+        wait_if(away, woslot(zz, yo, 0), wosem(zz, yo, 0))
+    wait_if(home, woslot(z, y, 0), wosem(z, y, 0))
+    wait_if(home, woslot(z, y, 1), wosem(z, y, 1))
+    for yy in (yn, yo):
+        arrived(woslot(z2, yy, 1), wosem(z2, yy, 1))
 
     gather_in(ap, ap_rs, apf_ss)
     gather_in(ad, ad_rs, adf_ss)
@@ -564,28 +667,6 @@
     decay_position_factor, decay_position_offset, head_norm_gain,
     pooling_output_weight, delta_output_weight,
 ):
-    def wide(rows):
-        rows = rows.astype(F32)
-        return jnp.pad(rows, ((0, 0), (0, 512 - rows.shape[1])))
-
-    def level(a):
-        return wide(jnp.broadcast_to(a[:, None], (2, 256)))
-
-    table = jnp.concatenate(
-        [
-            input_norm_gain.astype(F32).reshape(8, 512),
-            wide(decay_position_factor.T),
-            wide(decay_position_offset.T),
-            level(head_log_decay),
-            level(decay_logit_bias),
-            level(write_logit_bias),
-            wide(pooling_scale[None]),
-            jnp.zeros((5, 512), F32),
-            wide(head_norm_gain[None]),
-            jnp.zeros((7, 512), F32),
-        ],
-        axis=0,
-    )
     dma = pltpu.SemaphoreType.DMA
     vmem = pltpu.VMEM
     hbm = pl.BlockSpec(memory_space=pl.ANY)
@@ -593,17 +674,29 @@
     return pl.pallas_call(
         kernel,
         out_shape=jax.ShapeDtypeStruct((256, 512), BF16),
-        in_specs=[hbm] * 10 + [local] * 3,
+        in_specs=[hbm] * 19,
         out_specs=local,
         scratch_shapes=[
+            vmem((1, 2), F32),
+            vmem((1, 2), F32),
+            vmem((1, 2), F32),
+            vmem((8, 512), BF16),
+            vmem((2, 256), F32),
+            vmem((2, 256), F32),
+            vmem((1, 256), F32),
+            vmem((1, 128), F32),
+            vmem((32, 4096), BF16),
             vmem((8, 512, 512), BF16),
             vmem((32, 128, 768), BF16),
             vmem((4, 4, 512, 256), BF16),
-            vmem((2, 16, 512), F32),
+            vmem((8, 512), F32),
+            vmem((16, 256), F32),
+            vmem((2, 16, 256), F32),
             vmem((128, 128), BF16),
             vmem((512, 512), BF16),
             vmem((512, 768), F32),
             vmem((512, 128), F32),
+            vmem((128, 640), BF16),
             vmem((2, 128, 256), BF16),
             vmem((128, 256), BF16),
             vmem((4, 128, 256), BF16),
@@ -628,9 +721,9 @@
             vmem((256, 512), F32),
             vmem((256, 512), F32),
             vmem((128, 128), F32),
-            dma((16,)), dma((32,)), dma((16,)), dma((2,)), dma((1,)), dma((2,)),
+            dma((10,)), dma((1,)), dma((32,)), dma((32,)), dma((16,)), dma((2,)), dma((1,)), dma((2,)),
             dma((4,)), dma((1,)), dma((8,)), dma((8,)), dma((6,)),
-            dma((5,)), dma((13,)), dma((20,)), dma((32,)), dma((6,)), dma((28,)),
+            dma((10,)), dma((48,)), dma((41,)), dma((32,)), dma((10,)), dma((32,)),
             dma((2,)), dma((1,)), dma((1,)), dma((3,)), dma((1,)),
             dma((6,)), dma((6,)), dma((3,)), dma((3,)), dma((6,)),
         ],
@@ -639,8 +732,10 @@
         ),
     )(
         inputs, pooling_input_weight, query_weight, key_weight, value_weight,
-        gate_weight, pooling_output_weight, delta_output_weight, table,
-        pooling_group_map, table, decay_weight, strength_weight,
+        gate_weight, pooling_output_weight, delta_output_weight, pooling_group_map,
+        head_log_decay[None], decay_logit_bias[None], write_logit_bias[None],
+        input_norm_gain.reshape(8, 512), decay_position_factor.T, decay_position_offset.T,
+        pooling_scale[None], head_norm_gain[None], decay_weight.T, strength_weight.T,
     )
 
 

time: 100 us -> 84.8 us (0.85)
  local copies, waits for them, and re-layouts: 12.5 us -> 2.98 us
  Pallas kernels: 87.3 us -> 81.6 us
    pallas_call x1, Pallas kernels: 87.3 us -> 81.6 us  [per_device(): pl.pallas_call(kernel, out_shape=jax.ShapeDtypeStruct((256, 512), BF16),...]
    pad x7 -> x0, local copies, waits for them, and re-layouts: 2.77 us -> none  [wide(): return jnp.pad(rows, ((0, 0), (0, 512 - rows.shape[1])))]
    concatenate x1 -> x0, local copies, waits for them, and re-layouts: 2.47 us -> none  [per_device(): jnp.concatenate([input_norm_gain.astype(F32).reshape(8, 512), wide(decay_...]
    broadcast_in_dim x5 -> x0, local copies, waits for them, and re-layouts: 2.18 us -> none  [the longest x3 2.17 us: level(): return wide(jnp.broadcast_to(a[:, None], (2, 256)))]
    unnamed x7 -> x3, local copies, waits for them, and re-layouts: 4.37 us -> 2.37 us
where the time goes in v2:
time: 84.8 us; the launch traced here: 84.6 us
  Pallas kernels  81.6 us (96%)
  local copies, waits for them, and re-layouts  2.98 us (4%)
    pallas_call x1, Pallas kernels, per_device(): pl.pallas_call(kernel, out_shape=jax.ShapeDtypeStruct((256, 512), BF16),...  81.6 us
    unnamed x3, local copies, waits for them, and re-layouts  2.37 us

profile of v2, /device:TPU:1, one launch (start us, length us, event | category | flops | bytes accessed | tf_op | source)
XLA Modules:
  0.0 84.6 jit_solution(11427739052648279626)
XLA Ops:
  0.0 0.0 copy-start
  0.0 0.7 copy-done
  0.7 0.6 reshape.3.gain_in
  1.3 81.6 %shard_map.181 = bf16[256,512]{1,0:T(8,128)(2,1)} custom-call(bf16[256,512]{1,0:T(8,128)(2,1)} %x_in.1, bf16[256,256]{1,0:T(8,128)(2,1)} %wp_in.1, bf16[256,256]{1,0:T(8,128)(2,1)} %wq_in.1, bf16[256,256]{1,0:T(8,128)(2,1)} %wk_in.1, bf16[256,256]{1,0:T(8,128)(2,1)} %wv_in.1, bf16[256,256]{1,0:T(8,128)(2,1)} %wg_in.1, bf16[256,256]{1,0:T(8,128)(2,1)} %op_in.1, ...), custom_call_target="tpu_custom_call" | custom-call | tf_op jit(solution)/shard_map/pallas_call | solution.py:674
  82.9 1.7 %copy.21 = bf16[256,512]{1,0:T(8,128)(2,1)} copy(bf16[256,512]{1,0:T(8,128)(2,1)} %shard_map.181) | data formatting | bytes 524288
Async XLA Ops:
  0.0 0.7 copy-start

commit v3 on v2

v3 whole, which is shorter than its diff:
```python
import functools

import jax
import jax.numpy as jnp
from jax import lax
from jax.experimental import pallas as pl
from jax.experimental.pallas import tpu as pltpu
from jax.sharding import PartitionSpec as P

MESH = pl.DeviceIdType.MESH
F32 = jnp.float32
BF16 = jnp.bfloat16
HD = 128
EPS = 1e-06
HIGHEST = lax.Precision.HIGHEST


SCHEDULE = (
    ("TY",), ("TX",), ("TW",), ("OZ",), ("XA", 0), ("XR", "h", 3, 1), ("XR", "h", 1, 1),
    ("W0", 0), ("XR", "h", 1, 2), ("XB", 3), ("TS",), ("XA", 1), ("XO", 0), ("OXY",), ("W0", 3),
    ("WL", 1, 0), ("W0", 1), ("XB", 1), ("ST",), ("XR", "n", 1, 1), ("XA", 2), ("TB",),
    ("FILL",), ("WL", 3, 0), ("XR", "n", 3, 1), ("XN", 3), ("XR", "a", 1, 0), ("XR", "h", 3, 2),
    ("WL", 1, 3), ("XN", 0), ("XB2",), ("XN", 1), ("WL", 3, 1), ("XR", "n", 3, 2), ("W0", 2),
    ("OY",), ("XO", 1), ("XR", "h", 3, 0), ("XR", "h", 1, 0), ("XO", 2), ("WT", 3), ("XN", 2),
    ("WL", 3, 3), ("WL", 1, 1), ("XR", "n", 1, 0), ("WL", 3, 2), ("OB", 1), ("XR", "a", 1, 1),
    ("XR", "a", 3, 1), ("XR", "n", 3, 0), ("WL", 1, 2), ("XR", "n", 1, 2), ("OB", 3),
    ("XR", "a", 1, 2), ("XR", "a", 3, 0), ("OR", "h", 1), ("WT", 0), ("XR", "a", 3, 2),
    ("EARLY",), ("WT", 1), ("OR", "h", 3), ("WT", 2), ("OA",), ("ON", 0), ("LATE",), ("heads",),
    ("level", 1), ("level", 2), ("OB2",), ("level", 3), ("level", 4), ("level", 5),
    ("level", 6), ("OO",), ("level", 7), ("maps",), ("join",), ("OR", "n", 1), ("OR", "n", 3),
    ("ON", 3), ("ON", 1), ("pool",), ("state",), ("OR", "a", 3), ("OR", "a", 1), ("ON", 2),
    ("finish",), ("gather",), ("WOALL",),
)


def dot(a, b, dims=((1,), (0,)), precision=None):
    return lax.dot_general(
        a, b, (dims, ((), ())), precision=precision, preferred_element_type=F32
    )


def iota(shape, dim):
    return lax.broadcasted_iota(jnp.int32, shape, dim)


def silu(a):
    return a * jax.nn.sigmoid(a)


def unit(a):
    return a * lax.rsqrt(jnp.sum(a * a, axis=-1, keepdims=True) + EPS)


def kernel(
    x_in, wp_in, wq_in, wk_in, wv_in, wg_in, op_in, od_in, pm_in,
    hld_in, dlb_in, wlb_in, gain_in, factor_in, offset_in, pscale_in, hng_in, dw_in, sw_in,
    out_ref,
    hld_v, dlb_v, wlb_v, gain_v, factor_v, offset_v, pscale_v, hng_v, rates_v,
    xbuf, wbuf, wo, gain_f, pk_src, packb, pmb, xg, acc, ssq,
    w_stage, stc, stz_src, stz, pad, pool_src, delta_src, prev_src, ap, ad,
    rs2, rsp, rsm, rl, rin, o0, pmx, kw0_s, b0_s, keep_s, low_s, inv_s, up_s, down_s, state_s,
    in_rs, ws_rs, x_rs, w_rs, wo_rs, pk_rs, pm_rs, st_rs, stz_rs, prev_rs, ap_rs, ad_rs, rs_rs,
    x_ss, xf_ss, w_ss, wf_ss, wo_ss, wof_ss, pk_ss, pm_ss, st_ss, stz_ss, prev_ss,
    ap_ss, ad_ss, apf_ss, adf_ss, rs_ss,
):
    sp, tp = lax.axis_index("sp"), lax.axis_index("tp")
    z, y = lax.div(sp, 4), lax.rem(sp, 4)
    x, c = lax.div(tp, 2), lax.rem(tp, 2)
    kh = lax.div(y, 2)
    yodd = lax.rem(y, 2)
    home = c == kh
    away = jnp.logical_not(home)

    def mod4(a):
        return lax.rem(a + 8, 4)

    def dev(zz, yy, xx, cc):
        return (4 * zz + yy, 2 * xx + cc)

    zp, zm, z2 = mod4(z + 1), mod4(z - 1), mod4(z + 2)
    yp, ym = mod4(y + 1), mod4(y - 1)
    xp, xm, x2 = mod4(x + 1), mod4(x - 1), mod4(x + 2)
    me_z, me_y, me_x = z, y, x
    partner = dev(z, y, x, 1 - c)

    ends = []

    def remote(src, dst, ssem, rsem, to, cond=None):
        def make():
            return pltpu.make_async_remote_copy(
                src_ref=src, dst_ref=dst, send_sem=ssem, recv_sem=rsem,
                device_id=to, device_id_type=MESH,
            )

        if cond is None:
            make().start()
            ends.append(lambda: make().wait_send())
        else:
            @pl.when(cond)
            def _():
                make().start()

            def end():
                @pl.when(cond)
                def _():
                    make().wait_send()

            ends.append(end)

    def arrived(ref, sem):
        pltpu.make_async_copy(ref, ref, sem).wait()

    loads = [
        (hld_in, hld_v), (dlb_in, dlb_v), (wlb_in, wlb_v), (factor_in, factor_v),
        (offset_in, offset_v), (pscale_in, pscale_v), (gain_in, gain_v), (hng_in, hng_v),
        (dw_in, rates_v.at[pl.ds(0, 16), :]), (sw_in, rates_v.at[pl.ds(16, 16), :]),
    ]
    for i, (src, dst) in enumerate(loads):
        pltpu.make_async_copy(src, dst, in_rs.at[i]).start()

    barrier = pltpu.get_barrier_semaphore()
    peers = [partner]
    for d in (1, 2, 3):
        for cc in (0, 1):
            peers.append(dev(mod4(z + d), y, x, cc))
            peers.append(dev(z, mod4(y + d), x, cc))
            peers.append(dev(z, y, mod4(x + d), cc))
    for to in peers:
        pl.semaphore_signal(barrier, inc=1, device_id=to, device_id_type=MESH)
    pl.semaphore_wait(barrier, len(peers))

    def xslot(yy, xx, u, quarter=None):
        start, size = 128 * (u % 2), 128
        if quarter is not None:
            start, size = start + 64 * quarter, 64
        return xbuf.at[2 * xx + u // 2, pl.ds(256 * lax.rem(yy, 2) + start, size), :]

    def xsem(yy, xx, u):
        return x_rs.at[16 * lax.rem(yy, 2) + 4 * xx + u]

    def wslot(zz, yy, r):
        return wbuf.at[2 * (4 * zz + yy) + r, :, pl.ds(0, 640)]

    def wsem(zz, yy, r):
        return w_rs.at[2 * (4 * zz + yy) + r]

    def woslot(zz, yy, cc, half=None):
        block = wo.at[zz, 2 * lax.rem(yy, 2) + cc]
        return block if half is None else block.at[pl.ds(256 * half, 256), :]

    def wosem(zz, yy, cc):
        return wo_rs.at[4 * zz + 2 * lax.rem(yy, 2) + cc]

    def own_x(half):
        src = x_in.at[pl.ds(128 * half, 128), :]
        dst = xbuf.at[tp, pl.ds(256 * yodd + 128 * half, 128), :]
        return src, dst, x_rs.at[16 * yodd + 2 * tp + half]

    def own_x_along_y(half, cond=None):
        src, dst, sem = own_x(half)
        for i, yy in enumerate((yp, ym)):
            at = 6 + 2 * half + i
            remote(src, dst, x_ss.at[at], sem, dev(z, yy, x, kh), cond)

    def both(p, q):
        return jnp.logical_and(p, q)

    wo_own = wo.at[z, 2 * yodd + c]
    own_sem = wo_rs.at[4 * z + 2 * yodd + c]

    def own_wo(tos, at):
        for half, ref in enumerate((op_in, od_in)):
            part = wo_own.at[pl.ds(256 * half, 256), :]
            for i, to in enumerate(tos):
                remote(ref, part, wo_ss.at[at + 2 * half + i], own_sem, to)

    yn = 2 * c + 1 - yodd
    yo = 2 * c + yodd
    from_below = mod4(yn + 1) == y
    relay_half = jnp.where(from_below, 0, 1)
    y_next = jnp.where(from_below, yp, ym)
    xf_n, wf_n, wof_n = iter(range(64)), iter(range(64)), iter(range(64))
    x_ring = (dev(z, y, xp, c), dev(z, y, xm, c))
    y_ring = (dev(z, yp, x, c), dev(z, ym, x, c))
    z_ring = (dev(zp, y, x, c), dev(zm, y, x, c))
    y_relay = (relay_half, dev(z, y_next, x, c))
    x_relay = {3: (0, x_ring[0]), 1: (1, x_ring[1])}
    z_relay = {3: (0, z_ring[0]), 1: (1, z_ring[1])}
    x_at, z_at = (x, xp, x2, xm), (z, zp, z2, zm)
    cases = {"n": (yn, None), "h": (yo, home), "a": (yo, away)}
    seen = set()

    def take(key, slot, sem, cond=None):
        if key in seen:
            return
        seen.add(key)
        if cond is None:
            arrived(slot, sem)
        else:
            @pl.when(cond)
            def _():
                arrived(slot, sem)

    def x_take(case, d, u):
        yy, cond = cases[case]
        take(("x", case, d, u), xslot(yy, x_at[d], u), xsem(yy, x_at[d], u), cond)

    def x_pass(case, d, u, tos, relay=None):
        x_take(case, d, u)
        yy, cond = cases[case]
        slot, sem = xslot(yy, x_at[d], u), xsem(yy, x_at[d], u)
        for to in tos:
            remote(slot, slot, xf_ss.at[next(xf_n)], sem, to, cond)
        if relay is not None:
            half, to = relay
            part = xslot(yy, x_at[d], u, half)
            remote(part, part, xf_ss.at[next(xf_n)], sem, to, cond)

    def o_take(case, d, cc):
        yy, cond = cases[case]
        take(("o", case, d, cc), woslot(z_at[d], yy, cc), wosem(z_at[d], yy, cc), cond)

    def o_pass(case, d, cc, tos, relay=None):
        o_take(case, d, cc)
        yy, cond = cases[case]
        slot, sem = woslot(z_at[d], yy, cc), wosem(z_at[d], yy, cc)
        for to in tos:
            remote(slot, slot, wof_ss.at[next(wof_n)], sem, to, cond)
        if relay is not None:
            half, to = relay
            part = woslot(z_at[d], yy, cc, half)
            remote(part, part, wof_ss.at[next(wof_n)], sem, to, cond)

    def w_take(d, e, r, tag):
        yy = mod4(me_y + e)
        take((tag, d, e), wslot(z_at[d], yy, r), wsem(z_at[d], yy, r))

    def w_pass(d, e, tos):
        w_take(d, e, c, "w")
        yy = mod4(me_y + e)
        slot, sem = wslot(z_at[d], yy, c), wsem(z_at[d], yy, c)
        for to in (*tos, partner):
            remote(slot, slot, wf_ss.at[next(wf_n)], sem, to)

    def fill(i, carry):
        rows = pl.ds(pl.multiple_of(512 * i, 512), 512)
        both_cols = dot(rates_v[:, rows], pick, ((0,), (0,))).astype(BF16)
        wbuf[pl.ds(4 * i, 4), :, 640:768] = both_cols.reshape(4, 128, 128)
        return carry

    head = 4 * x + y
    row32, col32 = iota((32, 128), 0), iota((32, 128), 1)
    pick = jnp.logical_or(
        jnp.logical_and(row32 == head, col32 == 0),
        jnp.logical_and(row32 == head + 16, col32 == 1),
    ).astype(BF16)

    def project(i):
        gains = [gain_f[pl.ds(4 * i + q, 1), :] for q in range(4)]
        gain = jnp.concatenate(gains, axis=1)
        for b in range(4):
            rows = slice(128 * b, 128 * b + 128)
            v = xbuf[i, rows, :].astype(F32)
            sq = v * v
            ssq[rows, :] += (
                (sq[:, 0:128] + sq[:, 128:256]) + (sq[:, 256:384] + sq[:, 384:512])
            )
            xg[rows, :] = (v * gain).astype(BF16)
        acc[...] += dot(xg[...], wbuf[pl.ds(4 * i, 4)].reshape(512, 768))

    ii, jj = iota((256, 256), 0), iota((256, 256), 1)
    diff = jnp.bitwise_xor(ii, jj)
    lower = ii > jj
    causal = ii >= jj
    upto = (ii <= jj).astype(F32)
    eye = (ii == jj).astype(F32)

    def row_scale(b):
        total = jnp.sum(ssq[256 * b : 256 * b + 256, :], axis=-1, keepdims=True)
        return lax.rsqrt(total * (1.0 / 4096.0) + EPS)

    prev_to = dev(jnp.where(c == 0, z, zp), y, x, 1 - c)
    last = jnp.logical_and(z == 3, c == 1)
    first = jnp.logical_and(z == 0, c == 0)
    prev_dst = ap.at[pl.ds(256, 16), pl.ds(0, 128)]
    heads = []
    maps = []

    def spread_out(src, dst, rsem, ssem):
        cols = pl.ds(128 * y, 128)

        @pl.when(home)
        def _():
            dst[0:256, cols] = src[pl.ds(256 * yodd, 256), :]

        for j in (0, 1):
            to_y = 2 * c + j
            here = to_y == y
            rows = pl.ds(256 * j, 256)
            remote(
                src.at[rows, :], dst.at[pl.ds(0, 256), cols], ssem.at[3 * j],
                rsem.at[y], partner, here,
            )
            for r in (0, 1):
                remote(
                    src.at[pl.ds(256 * j + 128 * r, 128), :],
                    dst.at[pl.ds(128 * r, 128), cols],
                    ssem.at[3 * j + 1 + r], rsem.at[y], dev(z, to_y, x, r),
                    jnp.logical_not(here),
                )

    def gather_in(dst, rsem, fsem):
        for i, d in enumerate((1, 3, 2)):
            yy = mod4(me_y + d)
            part = dst.at[pl.ds(128 * c, 128), pl.ds(128 * yy, 128)]
            arrived(part, rsem.at[yy])
            remote(part, part, fsem.at[i], rsem.at[4 + yy], partner)
        for d in (1, 3, 2):
            yy = mod4(me_y + d)
            part = dst.at[pl.ds(128 * (1 - c), 128), pl.ds(128 * yy, 128)]
            arrived(part, rsem.at[4 + yy])

        @pl.when(away)
        def _():
            arrived(dst.at[pl.ds(0, 256), pl.ds(128 * me_y, 128)], rsem.at[me_y])

    def t_x():
        for half in (1, 0):
            src, dst, sem = own_x(half)
            for i, xx in enumerate((xp, xm)):
                remote(src, dst, x_ss.at[3 * half + i], sem, dev(z, y, xx, kh))
            remote(src, dst, x_ss.at[3 * half + 2], sem, partner, away)

            @pl.when(home)
            def _(src=src, dst=dst, sem=sem):
                pltpu.make_async_copy(src, dst, sem).start()

    def t_y():
        own_x_along_y(0)
        own_x_along_y(1, c == 0)

    def t_s():
        for j in (0, 1):
            same = yodd == j
            for r in (0, 1):
                far = dev(z, yp if r == 0 else ym, x, r)
                for n, ref in enumerate((wp_in, wq_in, wk_in, wv_in, wg_in)):
                    src = ref.at[pl.ds(128 * r, 128), pl.ds(128 * j, 128)]
                    dst = w_stage.at[:, pl.ds(128 * n, 128)]
                    remote(src, dst, w_ss.at[10 * j + 5 * r + n], ws_rs.at[0], far, both(away, same))

    def t_w():
        for j in (0, 1):
            same = yodd == j
            head_y = 2 * c + j
            for r in (0, 1):
                here = both(both(home, same), c == r)
                direct = jnp.logical_not(jnp.logical_or(here, both(away, same)))
                for n, ref in enumerate((wp_in, wq_in, wk_in, wv_in, wg_in)):
                    src = ref.at[pl.ds(128 * r, 128), pl.ds(128 * j, 128)]
                    dst = wbuf.at[2 * sp + r, :, pl.ds(128 * n, 128)]
                    remote(
                        src, dst, w_ss.at[20 + 10 * j + 5 * r + n], wsem(z, y, r),
                        dev(z, head_y, x, r), direct,
                    )

                    @pl.when(here)
                    def _(src=src, dst=dst, r=r):
                        pltpu.make_async_copy(src, dst, wsem(z, y, r)).start()

        for half, ref in enumerate((op_in, od_in)):
            part = wo_own.at[pl.ds(256 * half, 256), :]
            remote(ref, part, wo_ss.at[8 + half], own_sem, partner, away)

            @pl.when(home)
            def _(ref=ref, part=part):
                pltpu.make_async_copy(ref, part, own_sem).start()

    def t_b():
        for i, (src, dst) in enumerate(loads):
            pltpu.make_async_copy(src, dst, in_rs.at[i]).wait()
        pk_src[0:2, :] = factor_v[...]
        pk_src[2:4, :] = offset_v[...]
        for j in (0, 1):
            for at, ref in ((4, hld_v), (6, dlb_v), (8, wlb_v)):
                pk_src[at + j : at + j + 1, :] = jnp.broadcast_to(ref[0:1, j : j + 1], (1, 256))
        pk_src[10:11, :] = pscale_v[...]
        for j in (0, 1):
            head_y = 2 * c + j
            self_here = jnp.logical_and(head_y == y, home)
            remote(
                pk_src, packb.at[yodd], pk_ss.at[j], pk_rs.at[yodd], dev(z, head_y, x, kh),
                jnp.logical_not(self_here),
            )

            @pl.when(self_here)
            def _():
                packb[yodd] = pk_src[...]

        remote(pm_in.at[yodd], pmb, pm_ss.at[0], pm_rs.at[0], partner, home)

        @pl.when(home)
        def _():
            pltpu.make_async_copy(pm_in.at[yodd], pmb, pm_rs.at[0]).start()

    def stage():
        arrived(w_stage, ws_rs.at[0])
        stage_from = jnp.where(c == 0, ym, yp)
        stage_to = jnp.where(c == 0, yp, ym)
        stage_dst = wbuf.at[2 * (4 * z + stage_from) + c, :, pl.ds(0, 640)]
        remote(w_stage, stage_dst, w_ss.at[40], wsem(z, stage_from, c), dev(z, stage_to, x, c))

    def start_rates():
        lax.fori_loop(0, 8, fill, 0)
        gain_f[...] = gain_v[...].astype(F32)
        ssq[...] = jnp.zeros_like(ssq)
        acc[...] = jnp.zeros_like(acc)

    gap = mod4(x - z)

    def depth(parts, ds):
        for d in ds:
            for case in "nha":
                for u in range(4):
                    x_take(case, d, u)
            for e in (0, 1, 2, 3):
                w_take(d, e, c, "w")
                w_take(d, e, 1 - c, "p")
        for i in parts:
            lax.fori_loop(2 * i, 2 * i + 2, lambda k, carry: (project(k), carry)[1], 0)

    def early():
        first_part = jnp.where(gap == 2, xp, x)
        depth((first_part, jnp.where(gap == 2, xm, jnp.where(gap == 0, xp, z))), (0, 1, 3))

    def late():
        third = jnp.where(gap == 2, x, jnp.where(gap == 0, xm, x2))
        depth((third, jnp.where(gap == 2, z, jnp.where(gap == 0, x2, z2))), (2,))

    def delta_heads():
        for b in (0, 1):
            @pl.when(jnp.logical_or(away, yodd != b))
            def _(b=b):
                arrived(packb.at[b], pk_rs.at[b])
        arrived(pmb, pm_rs.at[0])

        scale = [row_scale(0), row_scale(1)]

        for b in (0, 1):
            pad[16 + 256 * b : 272 + 256 * b, :] = acc[256 * b : 256 * b + 256, 0:128] * scale[b]
        prev_src[...] = pad[512:528, :].astype(BF16)
        remote(prev_src, prev_dst, prev_ss.at[0], prev_rs.at[0], prev_to, jnp.logical_not(last))

        for b in (0, 1):
            rows = slice(256 * b, 256 * b + 256)
            s = scale[b]
            q = unit(silu(acc[rows, 128:256] * s)) * HD ** (-0.5)
            k = unit(silu(acc[rows, 256:384] * s))
            v = silu(acc[rows, 384:512] * s)
            rate = acc[rows, 640:768] * s
            table = packb[b]
            of = lambda r: jnp.where(yodd == 0, table[r : r + 1, :], table[r + 1 : r + 2, :])
            factor, offset, hld, dlb, wlb = (of(r) for r in (0, 2, 4, 6, 8))
            pre = rate.T[0:1, :] + dlb
            soft = jnp.maximum(pre, 0.0) + jnp.log1p(jnp.exp(-jnp.abs(pre)))
            log_decay = -jnp.exp(hld) * soft * factor + offset
            run_row = dot(jnp.broadcast_to(log_decay, (8, 256)), upto, precision=HIGHEST)[0:1, :]
            run = jnp.broadcast_to(run_row, (128, 256)).T
            beta = jax.nn.sigmoid(rate[:, 1:2] + wlb[:, 0:1])
            spread = jnp.concatenate([run, run], axis=1) - run_row
            decay = jnp.where(causal, jnp.exp(jnp.where(causal, spread, 0.0)), 0.0)
            k16, q16 = k.astype(BF16), q.astype(BF16)
            low = jnp.where(lower, dot(k16, k16, ((1,), (1,))) * (decay * beta), 0.0)
            scores = (dot(q16, k16, ((1,), (1,))) * decay).astype(BF16)
            inverse = eye - jnp.where(diff == 1, low, 0.0)
            grown = jnp.exp(run)
            kb = k * beta
            low_s[b] = low
            inv_s[b] = inverse
            heads.append(dict(q=q, k=k, v=v, scores=scores, run=run, grown=grown, kb=kb, beta=beta))

    def level_step(level):
        mask = jnp.right_shift(diff, level) == 1
        mids = []
        for b in (0, 1):
            off = jnp.where(mask, low_s[b], 0.0).astype(BF16)
            mids.append(dot(off, inv_s[b].astype(BF16)).astype(BF16))
        for b, mid in enumerate(mids):
            inv_s[b] = inv_s[b] - dot(inv_s[b].astype(BF16), mid)

    def delta_maps():
        for b, h in enumerate(heads):
            rows = slice(256 * b, 256 * b + 256)
            rhs = jnp.concatenate([h["v"] * h["beta"], h["kb"] * h["grown"]], axis=1)
            uw = rhs + dot((inv_s[b] - eye).astype(BF16), rhs.astype(BF16))
            uw16 = uw.astype(BF16)
            both = dot(h["scores"], uw16)
            o0[rows, :] = both[:, 0:128]
            pmx[rows, :] = (h["q"] * h["grown"] - both[:, 128:256]).astype(BF16)
            last_run = h["run"][255:256, :]
            kd = (h["k"] * jnp.exp(last_run - h["run"])).astype(BF16)
            ku = dot(kd, uw16, ((0,), (0,)))
            keep = jnp.exp(last_run)
            maps.append((keep, ku[:, 128:256].astype(BF16), ku[:, 0:128]))

        eye128 = (iota((128, 128), 0) == iota((128, 128), 1)).astype(F32)
        keep0, kw0, b0 = maps[0]
        keep1, kw1, b1 = maps[1]
        m0 = eye128 * keep0 - kw0.astype(F32)
        kw0_s[...] = kw0
        b0_s[...] = b0
        keep_s[0:1, :] = keep0
        first_map = jnp.concatenate([m0, b0], axis=1)
        keep1w = jnp.concatenate([keep1, keep1], axis=1)
        core_map = keep1w * first_map - dot(kw1, first_map.astype(BF16))
        core_map = core_map + jnp.concatenate([jnp.zeros_like(b1), b1], axis=1)
        stc[c] = core_map.astype(BF16)
        remote(stc.at[c], stc.at[c], st_ss.at[0], st_rs.at[c], partner)

    def join_maps():
        arrived(stc.at[1 - c], st_rs.at[1 - c])
        one = stc[1]
        chip_map = dot(one[:, 0:128], stc[0])
        chip_map = chip_map + jnp.concatenate([jnp.zeros((128, 128), F32), one[:, 128:256].astype(F32)], axis=1)
        stz_src[...] = chip_map.astype(BF16)
        for d in (1, 2, 3):
            remote(
                stz_src, stz.at[z], stz_ss.at[d - 1], stz_rs.at[z],
                dev(mod4(z + d), y, x, c), z + d <= 3,
            )

    def pool_part():
        @pl.when(first)
        def _():
            pad[0:16, :] = jnp.zeros((16, 128), F32)

        @pl.when(jnp.logical_not(first))
        def _():
            arrived(prev_dst, prev_rs.at[0])
            pad[0:16, :] = ap[256:272, 0:128].astype(F32)

        window = jnp.left_shift(2, y)
        base = 512 * (2 * z + c)
        for b in (0, 1):
            at = 256 * b
            sums = pad[16 + at : 272 + at, :]
            here = sums
            for lag in range(1, 16):
                part = pad[16 + at - lag : 272 + at - lag, :]
                sums = sums + part * jnp.where(lag < window, 1.0, 0.0)
            counts = jnp.minimum(base + at + iota((256, 128), 0) + 1, window).astype(F32)
            pooled = (sums / counts - here).astype(BF16)
            row = packb[b]
            pscale = jnp.where(yodd == 0, row[10:11, 0:128], row[10:11, 128:256])
            pool_src[at : at + 256, :] = (dot(pooled, pmb[...]) * pscale).astype(BF16)

        spread_out(pool_src, ap, ap_rs, ap_ss)

    def state_in():
        state_s[...] = jnp.zeros((128, 128), F32)

        def absorb(part):
            moved = dot(part[:, 0:128], state_s[...].astype(BF16))
            state_s[...] = moved + part[:, 128:256].astype(F32)

        for i in (0, 1, 2):
            @pl.when(i < z)
            def _(i=i):
                arrived(stz.at[i], stz_rs.at[i])
                absorb(stz[i])

        @pl.when(c == 1)
        def _():
            absorb(stc[0])

    def finish():
        hng = hng_v[...]
        for b in (0, 1):
            rows = slice(256 * b, 256 * b + 256)
            s16 = state_s[...].astype(BF16)
            o = o0[rows, :] + dot(pmx[rows, :], s16)
            gate = silu(acc[rows, 512:640] * row_scale(b))
            norm = lax.rsqrt(jnp.mean(o * o, axis=-1, keepdims=True) + EPS)
            delta_src[rows, :] = (o * norm * hng * gate).astype(BF16)
            if b == 0:
                state_s[...] = keep_s[0:1, :] * state_s[...] - dot(kw0_s[...], s16) + b0_s[...]

        spread_out(delta_src, ad, ad_rs, ad_ss)

    def gather_both():
        gather_in(ap, ap_rs, apf_ss)
        gather_in(ad, ad_rs, adf_ss)

    def rest_of_output_weights():
        for d in range(4):
            for case in "nha":
                for cc in (0, 1):
                    o_take(case, d, cc)

    ops = dict(
        TX=t_x, gather=gather_both, TY=t_y, TS=t_s, TW=t_w, TB=t_b, ST=stage, FILL=start_rates, EARLY=early,
        LATE=late, heads=delta_heads, level=level_step, maps=delta_maps, join=join_maps,
        pool=pool_part, state=state_in, finish=finish, WOALL=rest_of_output_weights,
        W0=lambda e: w_pass(0, e, z_ring),
        WL=lambda d, e: w_pass(d, e, (z_relay[d][1],) if (d == 3) == (e in (0, 2)) else ()),
        WT=lambda e: w_pass(2, e, ()),
        XA=lambda u: x_pass("n", 0, u, x_ring, y_relay),
        XO=lambda u: x_pass("a", 0, u, x_ring),
        XB=lambda d: x_pass("h", d, 3, y_ring, x_relay[d]),
        XB2=lambda: x_pass("h", 2, 3, y_ring),
        XN=lambda d: x_pass("n", d, 3, (), y_relay),
        XR=lambda case, d, u: x_pass(case, d, u, (), x_relay[d]),
        OXY=lambda: own_x_along_y(1, c == 1),
        OY=lambda: own_wo((dev(z, yp, x, kh), dev(z, ym, x, kh)), 4),
        OZ=lambda: own_wo((dev(zp, y, x, kh), dev(zm, y, x, kh)), 0),
        OA=lambda: o_pass("n", 0, 1, z_ring, y_relay),
        OO=lambda: o_pass("a", 0, 1, z_ring),
        OB=lambda d: o_pass("h", d, 0, y_ring, z_relay[d]),
        OB2=lambda: o_pass("h", 2, 0, y_ring),
        ON=lambda d: o_pass("n", d, 0, (), y_relay),
        OR=lambda case, d: o_pass(case, d, 1, (), z_relay[d]),
    )
    for name, *args in SCHEDULE:
        ops[name](*args)

    def piece(zz):
        halves = []
        for j in (0, 1):
            part = None
            for cc in (0, 1):
                cols = slice(256 * cc, 256 * cc + 256)
                term = dot(ap[0:256, cols], wo[zz, 2 * j + cc, 0:256, :])
                term = term + dot(ad[0:256, cols], wo[zz, 2 * j + cc, 256:512, :])
                part = term if part is None else part + term
            halves.append(part)
        return jnp.concatenate(halves, axis=1)

    top, bottom = pl.ds(0, 128), pl.ds(128, 128)
    to_p, to_m = dev(z, y, xp, c), dev(z, y, xm, c)
    rs2[...] = piece(x2).astype(BF16)
    remote(rs2.at[top, :], rl.at[0], rs_ss.at[0], rs_rs.at[0], to_p)
    remote(rs2.at[bottom, :], rl.at[1], rs_ss.at[1], rs_rs.at[1], to_m)
    up_s[...] = piece(xp)
    rsp[128:256, :] = up_s[128:256, :].astype(BF16)
    remote(rsp.at[bottom, :], rin.at[0, bottom, :], rs_ss.at[2], rs_rs.at[2], to_p)
    down_s[...] = piece(xm)
    rsm[0:128, :] = down_s[0:128, :].astype(BF16)
    remote(rsm.at[top, :], rin.at[1, top, :], rs_ss.at[3], rs_rs.at[3], to_m)
    arrived(rl.at[0], rs_rs.at[0])
    rsp[0:128, :] = (up_s[0:128, :] + rl[0].astype(F32)).astype(BF16)
    remote(rsp.at[top, :], rin.at[0, top, :], rs_ss.at[4], rs_rs.at[4], to_p)
    arrived(rl.at[1], rs_rs.at[1])
    rsm[128:256, :] = (down_s[128:256, :] + rl[1].astype(F32)).astype(BF16)
    remote(rsm.at[bottom, :], rin.at[1, bottom, :], rs_ss.at[5], rs_rs.at[5], to_m)
    mine = piece(x)
    arrived(rin.at[0, bottom, :], rs_rs.at[2])
    arrived(rin.at[1, top, :], rs_rs.at[3])
    arrived(rin.at[0, top, :], rs_rs.at[4])
    arrived(rin.at[1, bottom, :], rs_rs.at[5])
    out_ref[...] = (mine + rin[0].astype(F32) + rin[1].astype(F32)).astype(BF16)

    for end in ends:
        end()


def per_device(
    inputs, input_norm_gain, pooling_input_weight, query_weight, key_weight,
    value_weight, gate_weight, decay_weight, strength_weight, pooling_group_map,
    pooling_scale, head_log_decay, decay_logit_bias, write_logit_bias,
    decay_position_factor, decay_position_offset, head_norm_gain,
    pooling_output_weight, delta_output_weight,
):
    dma = pltpu.SemaphoreType.DMA
    vmem = pltpu.VMEM
    hbm = pl.BlockSpec(memory_space=pl.ANY)
    local = pl.BlockSpec(memory_space=pltpu.VMEM)
    return pl.pallas_call(
        kernel,
        out_shape=pltpu.VMEM((256, 512), BF16),
        in_specs=[hbm] * 19,
        out_specs=local,
        scratch_shapes=[
            vmem((1, 2), F32),
            vmem((1, 2), F32),
            vmem((1, 2), F32),
            vmem((32, 128), BF16),
            vmem((2, 256), F32),
            vmem((2, 256), F32),
            vmem((1, 256), F32),
            vmem((1, 128), F32),
            vmem((32, 4096), BF16),
            vmem((8, 512, 512), BF16),
            vmem((32, 128, 768), BF16),
            vmem((4, 4, 512, 256), BF16),
            vmem((32, 128), F32),
            vmem((16, 256), F32),
            vmem((2, 16, 256), F32),
            vmem((128, 128), BF16),
            vmem((512, 512), BF16),
            vmem((512, 768), F32),
            vmem((512, 128), F32),
            vmem((128, 640), BF16),
            vmem((2, 128, 256), BF16),
            vmem((128, 256), BF16),
            vmem((4, 128, 256), BF16),
            vmem((528, 128), F32),
            vmem((512, 128), BF16),
            vmem((512, 128), BF16),
            vmem((16, 128), BF16),
            vmem((272, 512), BF16),
            vmem((256, 512), BF16),
            vmem((256, 512), BF16),
            vmem((256, 512), BF16),
            vmem((256, 512), BF16),
            vmem((2, 128, 512), BF16),
            vmem((2, 256, 512), BF16),
            vmem((512, 128), F32),
            vmem((512, 128), BF16),
            vmem((128, 128), BF16),
            vmem((128, 128), F32),
            vmem((8, 128), F32),
            vmem((2, 256, 256), F32),
            vmem((2, 256, 256), F32),
            vmem((256, 512), F32),
            vmem((256, 512), F32),
            vmem((128, 128), F32),
            dma((10,)), dma((1,)), dma((32,)), dma((32,)), dma((16,)), dma((2,)), dma((1,)), dma((2,)),
            dma((4,)), dma((1,)), dma((8,)), dma((8,)), dma((6,)),
            dma((10,)), dma((48,)), dma((41,)), dma((32,)), dma((10,)), dma((32,)),
            dma((2,)), dma((1,)), dma((1,)), dma((3,)), dma((1,)),
            dma((6,)), dma((6,)), dma((3,)), dma((3,)), dma((6,)),
        ],
        compiler_params=pltpu.CompilerParams(
            collective_id=0, has_side_effects=True, vmem_limit_bytes=60 * 1024 * 1024
        ),
    )(
        inputs, pooling_input_weight, query_weight, key_weight, value_weight,
        gate_weight, pooling_output_weight, delta_output_weight, pooling_group_map,
        head_log_decay[None], decay_logit_bias[None], write_logit_bias[None],
        input_norm_gain.reshape(32, 128), decay_position_factor.T, decay_position_offset.T,
        pooling_scale[None], head_norm_gain[None], decay_weight.T, strength_weight.T,
    )


def solution(mesh):
    rows, heads = P("sp", "tp"), P("tp")
    in_specs = (
        rows, P(), rows, rows, rows, rows, rows, P(), P(), P("tp", None, None),
        heads, heads, heads, heads, rows, rows, P(), P("tp", "sp"), P("tp", "sp"),
    )
    return jax.shard_map(
        per_device, mesh=mesh, in_specs=in_specs, out_specs=rows, check_vma=False
    )
```

time: 84.8 us -> 75.8 us (0.89)
  Pallas kernels: 81.6 us -> 74.9 us
  local copies, waits for them, and re-layouts: 2.98 us -> 0.71 us
    pallas_call x1, Pallas kernels: 81.6 us -> 74.9 us  [per_device(): pl.pallas_call(kernel, out_shape=pltpu.VMEM((256, 512), BF16), in_specs=[...]
    unnamed x3 -> x1, local copies, waits for them, and re-layouts: 2.37 us -> 0.71 us
where the time goes in v3:
time: 75.8 us; the launch traced here: 75.6 us
  Pallas kernels  74.9 us (99%)
    pallas_call x1, Pallas kernels, per_device(): pl.pallas_call(kernel, out_shape=pltpu.VMEM((256, 512), BF16), in_specs=[...  74.9 us

profile of v3, /device:TPU:1, one launch (start us, length us, event | category | flops | bytes accessed | tf_op | source)
XLA Modules:
  0.0 75.6 jit_solution(11421134217838318048)
XLA Ops:
  0.0 74.9 %shard_map.181 = bf16[256,512]{1,0:T(8,128)(2,1)S(1)} custom-call(bf16[256,512]{1,0:T(8,128)(2,1)} %x_in.1, bf16[256,256]{1,0:T(8,128)(2,1)} %wp_in.1, bf16[256,256]{1,0:T(8,128)(2,1)} %wq_in.1, bf16[256,256]{1,0:T(8,128)(2,1)} %wk_in.1, bf16[256,256]{1,0:T(8,128)(2,1)} %wv_in.1, bf16[256,256]{1,0:T(8,128)(2,1)} %wg_in.1, bf16[256,256]{1,0:T(8,128)(2,1)} %op_in.1, ...), custom_call_target="tpu_custom_call" | custom-call | tf_op jit(solution)/shard_map/pallas_call | solution.py:677
  74.9 0.7 copy.21

commit v4 on v3

--- a/solution.py
+++ b/solution.py
@@ -12,24 +12,26 @@
 BF16 = jnp.bfloat16
 HD = 128
 EPS = 1e-06
+PARTS = ((0, 128), (128, 128), (0, 128), (128, 128))
 HIGHEST = lax.Precision.HIGHEST
 
 
 SCHEDULE = (
-    ("TY",), ("TX",), ("TW",), ("OZ",), ("XA", 0), ("XR", "h", 3, 1), ("XR", "h", 1, 1),
-    ("W0", 0), ("XR", "h", 1, 2), ("XB", 3), ("TS",), ("XA", 1), ("XO", 0), ("OXY",), ("W0", 3),
-    ("WL", 1, 0), ("W0", 1), ("XB", 1), ("ST",), ("XR", "n", 1, 1), ("XA", 2), ("TB",),
-    ("FILL",), ("WL", 3, 0), ("XR", "n", 3, 1), ("XN", 3), ("XR", "a", 1, 0), ("XR", "h", 3, 2),
-    ("WL", 1, 3), ("XN", 0), ("XB2",), ("XN", 1), ("WL", 3, 1), ("XR", "n", 3, 2), ("W0", 2),
-    ("OY",), ("XO", 1), ("XR", "h", 3, 0), ("XR", "h", 1, 0), ("XO", 2), ("WT", 3), ("XN", 2),
-    ("WL", 3, 3), ("WL", 1, 1), ("XR", "n", 1, 0), ("WL", 3, 2), ("OB", 1), ("XR", "a", 1, 1),
-    ("XR", "a", 3, 1), ("XR", "n", 3, 0), ("WL", 1, 2), ("XR", "n", 1, 2), ("OB", 3),
-    ("XR", "a", 1, 2), ("XR", "a", 3, 0), ("OR", "h", 1), ("WT", 0), ("XR", "a", 3, 2),
-    ("EARLY",), ("WT", 1), ("OR", "h", 3), ("WT", 2), ("OA",), ("ON", 0), ("LATE",), ("heads",),
-    ("level", 1), ("level", 2), ("OB2",), ("level", 3), ("level", 4), ("level", 5),
-    ("level", 6), ("OO",), ("level", 7), ("maps",), ("join",), ("OR", "n", 1), ("OR", "n", 3),
-    ("ON", 3), ("ON", 1), ("pool",), ("state",), ("OR", "a", 3), ("OR", "a", 1), ("ON", 2),
-    ("finish",), ("gather",), ("WOALL",),
+    ("TX",), ("TY",), ("TW",), ("OZ",), ("XR", "h", 3, 1), ("XA", 0), ("W0", 0),
+    ("XR", "h", 1, 2), ("XB", 3), ("XR", "h", 1, 1), ("TS",), ("XA", 1), ("XO", 0), ("W0", 3),
+    ("XB", 1), ("OXY",), ("W0", 1), ("ST",), ("XA", 2), ("TB",), ("FILL",), ("XN", 3),
+    ("XR", "n", 1, 1), ("XR", "n", 3, 1), ("XR", "h", 3, 2), ("WL", 3, 0), ("XO", 1),
+    ("WL", 1, 3), ("XN", 1), ("XB2",), ("XR", "a", 1, 0), ("W0", 2), ("XR", "n", 3, 2),
+    ("XN", 0), ("XO", 2), ("WL", 1, 1), ("WL", 1, 0), ("OR", "h", 3), ("OY",), ("XN", 2),
+    ("XR", "a", 3, 1), ("WT", 3), ("WL", 3, 3), ("XR", "h", 1, 0), ("XR", "a", 1, 1),
+    ("XR", "a", 3, 0), ("WL", 3, 1), ("OB", 1), ("XR", "n", 1, 0), ("OR", "h", 1),
+    ("XR", "a", 1, 2), ("WL", 1, 2), ("XR", "n", 3, 0), ("WL", 3, 2), ("XR", "h", 3, 0),
+    ("XR", "n", 1, 2), ("XR", "a", 3, 2), ("WT", 0), ("OB", 3), ("EARLY",), ("WT", 1),
+    ("WT", 2), ("OA",), ("LATEX",), ("LATE",), ("heads",), ("ON", 1), ("level", 1), ("ON", 0),
+    ("level", 2), ("OO",), ("OB2",), ("level", 3), ("level", 4), ("level", 5), ("level", 6),
+    ("level", 7), ("maps",), ("join",), ("ON", 3), ("OR", "n", 3), ("OR", "a", 1),
+    ("OR", "a", 3), ("pool",), ("ON", 2), ("OR", "n", 1), ("state",), ("finish",), ("GP",),
+    ("GD",), ("WOALL",),
 )
 
 
@@ -55,11 +57,11 @@
     x_in, wp_in, wq_in, wk_in, wv_in, wg_in, op_in, od_in, pm_in,
     hld_in, dlb_in, wlb_in, gain_in, factor_in, offset_in, pscale_in, hng_in, dw_in, sw_in,
     out_ref,
-    hld_v, dlb_v, wlb_v, gain_v, factor_v, offset_v, pscale_v, hng_v, rates_v,
+    hld_v, dlb_v, wlb_v, gain_v, factor_v, offset_v, pscale_v, hng_v, rates_v, x_v, w_v, wo_v,
     xbuf, wbuf, wo, gain_f, pk_src, packb, pmb, xg, acc, ssq,
     w_stage, stc, stz_src, stz, pad, pool_src, delta_src, prev_src, ap, ad,
     rs2, rsp, rsm, rl, rin, o0, pmx, kw0_s, b0_s, keep_s, low_s, inv_s, up_s, down_s, state_s,
-    in_rs, ws_rs, x_rs, w_rs, wo_rs, pk_rs, pm_rs, st_rs, stz_rs, prev_rs, ap_rs, ad_rs, rs_rs,
+    in_rs, big_rs, near, ws_rs, x_rs, w_rs, wo_rs, pk_rs, pm_rs, st_rs, stz_rs, prev_rs, ap_rs, ad_rs, rs_rs,
     x_ss, xf_ss, w_ss, wf_ss, wo_ss, wof_ss, pk_ss, pm_ss, st_ss, stz_ss, prev_ss,
     ap_ss, ad_ss, apf_ss, adf_ss, rs_ss,
 ):
@@ -115,12 +117,17 @@
         (offset_in, offset_v), (pscale_in, pscale_v), (gain_in, gain_v), (hng_in, hng_v),
         (dw_in, rates_v.at[pl.ds(0, 16), :]), (sw_in, rates_v.at[pl.ds(16, 16), :]),
     ]
+    big = [(x_in, x_v)]
+    big += [(ref, w_v.at[n]) for n, ref in enumerate((wp_in, wq_in, wk_in, wv_in, wg_in))]
+    big += [(ref, wo_v.at[n]) for n, ref in enumerate((op_in, od_in))]
+    for i, (src, dst) in enumerate(big):
+        pltpu.make_async_copy(src, dst, big_rs.at[i]).start()
     for i, (src, dst) in enumerate(loads):
         pltpu.make_async_copy(src, dst, in_rs.at[i]).start()
 
     barrier = pltpu.get_barrier_semaphore()
     peers = [partner]
-    for d in (1, 2, 3):
+    for d in (1, 3):
         for cc in (0, 1):
             peers.append(dev(mod4(z + d), y, x, cc))
             peers.append(dev(z, mod4(y + d), x, cc))
@@ -128,11 +135,15 @@
     for to in peers:
         pl.semaphore_signal(barrier, inc=1, device_id=to, device_id_type=MESH)
     pl.semaphore_wait(barrier, len(peers))
+    for to in (dev(zp, y, x, c), dev(zm, y, x, c), dev(z, yp, x, c), dev(z, ym, x, c)):
+        pl.semaphore_signal(near, inc=1, device_id=to, device_id_type=MESH)
+    for i, (src, dst) in enumerate(big):
+        pltpu.make_async_copy(src, dst, big_rs.at[i]).wait()
 
     def xslot(yy, xx, u, quarter=None):
-        start, size = 128 * (u % 2), 128
+        start, size = PARTS[u]
         if quarter is not None:
-            start, size = start + 64 * quarter, 64
+            start, size = start + size // 2 * quarter, size // 2
         return xbuf.at[2 * xx + u // 2, pl.ds(256 * lax.rem(yy, 2) + start, size), :]
 
     def xsem(yy, xx, u):
@@ -151,16 +162,14 @@
     def wosem(zz, yy, cc):
         return wo_rs.at[4 * zz + 2 * lax.rem(yy, 2) + cc]
 
-    def own_x(half):
-        src = x_in.at[pl.ds(128 * half, 128), :]
-        dst = xbuf.at[tp, pl.ds(256 * yodd + 128 * half, 128), :]
-        return src, dst, x_rs.at[16 * yodd + 2 * tp + half]
-
-    def own_x_along_y(half, cond=None):
-        src, dst, sem = own_x(half)
+    def own_x(u):
+        start, size = PARTS[u]
+        return x_v.at[pl.ds(start, size), :], xslot(y, x, u), xsem(y, x, u)
+
+    def own_x_along_y(u):
+        src, dst, sem = own_x(u)
         for i, yy in enumerate((yp, ym)):
-            at = 6 + 2 * half + i
-            remote(src, dst, x_ss.at[at], sem, dev(z, yy, x, kh), cond)
+            remote(src, dst, x_ss.at[12 + 2 * u + i], sem, dev(z, yy, x, kh), c == u // 2)
 
     def both(p, q):
         return jnp.logical_and(p, q)
@@ -172,7 +181,7 @@
         for half, ref in enumerate((op_in, od_in)):
             part = wo_own.at[pl.ds(256 * half, 256), :]
             for i, to in enumerate(tos):
-                remote(ref, part, wo_ss.at[at + 2 * half + i], own_sem, to)
+                remote(wo_v.at[half], part, wo_ss.at[at + 2 * half + i], own_sem, to)
 
     yn = 2 * c + 1 - yodd
     yo = 2 * c + yodd
@@ -256,17 +265,20 @@
     ).astype(BF16)
 
     def project(i):
-        gains = [gain_f[pl.ds(4 * i + q, 1), :] for q in range(4)]
-        gain = jnp.concatenate(gains, axis=1)
-        for b in range(4):
-            rows = slice(128 * b, 128 * b + 128)
-            v = xbuf[i, rows, :].astype(F32)
-            sq = v * v
-            ssq[rows, :] += (
-                (sq[:, 0:128] + sq[:, 128:256]) + (sq[:, 256:384] + sq[:, 384:512])
-            )
-            xg[rows, :] = (v * gain).astype(BF16)
-        acc[...] += dot(xg[...], wbuf[pl.ds(4 * i, 4)].reshape(512, 768))
+        total = acc[...]
+        for k in (0, 1):
+            gains = [gain_f[pl.ds(8 * i + 4 * k + q, 1), :] for q in range(4)]
+            gain = jnp.concatenate(gains, axis=1)
+            for b in range(4):
+                rows = slice(128 * b, 128 * b + 128)
+                v = xbuf[2 * i + k, rows, :].astype(F32)
+                sq = v * v
+                ssq[rows, :] += (
+                    (sq[:, 0:128] + sq[:, 128:256]) + (sq[:, 256:384] + sq[:, 384:512])
+                )
+                xg[k, rows, :] = (v * gain).astype(BF16)
+            total = total + dot(xg[k], wbuf[pl.ds(8 * i + 4 * k, 4)].reshape(512, 768))
+        acc[...] = total
 
     ii, jj = iota((256, 256), 0), iota((256, 256), 1)
     diff = jnp.bitwise_xor(ii, jj)
@@ -309,35 +321,24 @@
                     jnp.logical_not(here),
                 )
 
-    def gather_in(dst, rsem, fsem):
-        for i, d in enumerate((1, 3, 2)):
-            yy = mod4(me_y + d)
-            part = dst.at[pl.ds(128 * c, 128), pl.ds(128 * yy, 128)]
-            arrived(part, rsem.at[yy])
-            remote(part, part, fsem.at[i], rsem.at[4 + yy], partner)
-        for d in (1, 3, 2):
-            yy = mod4(me_y + d)
-            part = dst.at[pl.ds(128 * (1 - c), 128), pl.ds(128 * yy, 128)]
-            arrived(part, rsem.at[4 + yy])
-
-        @pl.when(away)
-        def _():
-            arrived(dst.at[pl.ds(0, 256), pl.ds(128 * me_y, 128)], rsem.at[me_y])
-
     def t_x():
         for half in (1, 0):
-            src, dst, sem = own_x(half)
-            for i, xx in enumerate((xp, xm)):
-                remote(src, dst, x_ss.at[3 * half + i], sem, dev(z, y, xx, kh))
-            remote(src, dst, x_ss.at[3 * half + 2], sem, partner, away)
-
-            @pl.when(home)
-            def _(src=src, dst=dst, sem=sem):
-                pltpu.make_async_copy(src, dst, sem).start()
+            for cc in (0, 1):
+                u = 2 * cc + half
+                src, dst, sem = own_x(u)
+                for i, xx in enumerate((xp, xm)):
+                    remote(src, dst, x_ss.at[3 * u + i], sem, dev(z, y, xx, kh), c == cc)
+                mine = c == cc
+                remote(src, dst, x_ss.at[3 * u + 2], sem, partner, both(mine, away))
+
+                @pl.when(both(mine, home))
+                def _(u=u, dst=dst, sem=sem):
+                    start, size = PARTS[u]
+                    pltpu.make_async_copy(x_in.at[pl.ds(start, size), :], dst, sem).start()
 
     def t_y():
-        own_x_along_y(0)
-        own_x_along_y(1, c == 0)
+        for u in (0, 1, 2):
+            own_x_along_y(u)
 
     def t_s():
         for j in (0, 1):
@@ -345,7 +346,7 @@
             for r in (0, 1):
                 far = dev(z, yp if r == 0 else ym, x, r)
                 for n, ref in enumerate((wp_in, wq_in, wk_in, wv_in, wg_in)):
-                    src = ref.at[pl.ds(128 * r, 128), pl.ds(128 * j, 128)]
+                    src = w_v.at[n, pl.ds(128 * r, 128), pl.ds(128 * j, 128)]
                     dst = w_stage.at[:, pl.ds(128 * n, 128)]
                     remote(src, dst, w_ss.at[10 * j + 5 * r + n], ws_rs.at[0], far, both(away, same))
 
@@ -359,8 +360,9 @@
                 for n, ref in enumerate((wp_in, wq_in, wk_in, wv_in, wg_in)):
                     src = ref.at[pl.ds(128 * r, 128), pl.ds(128 * j, 128)]
                     dst = wbuf.at[2 * sp + r, :, pl.ds(128 * n, 128)]
+                    here_v = w_v.at[n, pl.ds(128 * r, 128), pl.ds(128 * j, 128)]
                     remote(
-                        src, dst, w_ss.at[20 + 10 * j + 5 * r + n], wsem(z, y, r),
+                        here_v, dst, w_ss.at[20 + 10 * j + 5 * r + n], wsem(z, y, r),
                         dev(z, head_y, x, r), direct,
                     )
 
@@ -370,7 +372,7 @@
 
         for half, ref in enumerate((op_in, od_in)):
             part = wo_own.at[pl.ds(256 * half, 256), :]
-            remote(ref, part, wo_ss.at[8 + half], own_sem, partner, away)
+            remote(wo_v.at[half], part, wo_ss.at[8 + half], own_sem, partner, away)
 
             @pl.when(home)
             def _(ref=ref, part=part):
@@ -427,15 +429,20 @@
                 w_take(d, e, c, "w")
                 w_take(d, e, 1 - c, "p")
         for i in parts:
-            lax.fori_loop(2 * i, 2 * i + 2, lambda k, carry: (project(k), carry)[1], 0)
+            project(i)
 
     def early():
         first_part = jnp.where(gap == 2, xp, x)
         depth((first_part, jnp.where(gap == 2, xm, jnp.where(gap == 0, xp, z))), (0, 1, 3))
 
+    def late_x():
+        for case in "nha":
+            for u in range(4):
+                x_take(case, 2, u)
+        project(jnp.where(gap == 0, xm, jnp.where(gap == 2, z, x2)))
+
     def late():
-        third = jnp.where(gap == 2, x, jnp.where(gap == 0, xm, x2))
-        depth((third, jnp.where(gap == 2, z, jnp.where(gap == 0, x2, z2))), (2,))
+        depth((jnp.where(gap == 0, x2, jnp.where(gap == 2, x, z2)),), (2,))
 
     def delta_heads():
         for b in (0, 1):
@@ -523,7 +530,8 @@
         chip_map = dot(one[:, 0:128], stc[0])
         chip_map = chip_map + jnp.concatenate([jnp.zeros((128, 128), F32), one[:, 128:256].astype(F32)], axis=1)
         stz_src[...] = chip_map.astype(BF16)
-        for d in (1, 2, 3):
+        pl.semaphore_wait(near, 4)
+        for d in (2, 1, 3):
             remote(
                 stz_src, stz.at[z], stz_ss.at[d - 1], stz_rs.at[z],
                 dev(mod4(z + d), y, x, c), z + d <= 3,
@@ -587,19 +595,35 @@
 
         spread_out(delta_src, ad, ad_rs, ad_ss)
 
-    def gather_both():
-        gather_in(ap, ap_rs, apf_ss)
-        gather_in(ad, ad_rs, adf_ss)
+    def pass_on(dst, rsem, fsem):
+        for i, d in enumerate((1, 3, 2)):
+            yy = mod4(me_y + d)
+            part = dst.at[pl.ds(128 * c, 128), pl.ds(128 * yy, 128)]
+            arrived(part, rsem.at[yy])
+            remote(part, part, fsem.at[i], rsem.at[4 + yy], partner)
+
+    def from_partner(dst, rsem):
+        for d in (1, 3, 2):
+            yy = mod4(me_y + d)
+            part = dst.at[pl.ds(128 * (1 - c), 128), pl.ds(128 * yy, 128)]
+            arrived(part, rsem.at[4 + yy])
+
+        @pl.when(away)
+        def _():
+            arrived(dst.at[pl.ds(0, 256), pl.ds(128 * me_y, 128)], rsem.at[me_y])
 
     def rest_of_output_weights():
         for d in range(4):
             for case in "nha":
                 for cc in (0, 1):
                     o_take(case, d, cc)
+        from_partner(ap, ap_rs)
+        from_partner(ad, ad_rs)
 
     ops = dict(
-        TX=t_x, gather=gather_both, TY=t_y, TS=t_s, TW=t_w, TB=t_b, ST=stage, FILL=start_rates, EARLY=early,
-        LATE=late, heads=delta_heads, level=level_step, maps=delta_maps, join=join_maps,
+        TX=t_x, GP=lambda: pass_on(ap, ap_rs, apf_ss),
+        GD=lambda: pass_on(ad, ad_rs, adf_ss), TY=t_y, TS=t_s, TW=t_w, TB=t_b, ST=stage, FILL=start_rates, EARLY=early,
+        LATEX=late_x, LATE=late, heads=delta_heads, level=level_step, maps=delta_maps, join=join_maps,
         pool=pool_part, state=state_in, finish=finish, WOALL=rest_of_output_weights,
         W0=lambda e: w_pass(0, e, z_ring),
         WL=lambda d, e: w_pass(d, e, (z_relay[d][1],) if (d == 3) == (e in (0, 2)) else ()),
@@ -610,7 +634,7 @@
         XB2=lambda: x_pass("h", 2, 3, y_ring),
         XN=lambda d: x_pass("n", d, 3, (), y_relay),
         XR=lambda case, d, u: x_pass(case, d, u, (), x_relay[d]),
-        OXY=lambda: own_x_along_y(1, c == 1),
+        OXY=lambda: own_x_along_y(3),
         OY=lambda: own_wo((dev(z, yp, x, kh), dev(z, ym, x, kh)), 4),
         OZ=lambda: own_wo((dev(zp, y, x, kh), dev(zm, y, x, kh)), 0),
         OA=lambda: o_pass("n", 0, 1, z_ring, y_relay),
@@ -689,6 +713,9 @@
             vmem((1, 256), F32),
             vmem((1, 128), F32),
             vmem((32, 4096), BF16),
+            vmem((256, 512), BF16),
+            vmem((5, 256, 256), BF16),
+            vmem((2, 256, 256), BF16),
             vmem((8, 512, 512), BF16),
             vmem((32, 128, 768), BF16),
             vmem((4, 4, 512, 256), BF16),
@@ -696,7 +723,7 @@
             vmem((16, 256), F32),
             vmem((2, 16, 256), F32),
             vmem((128, 128), BF16),
-            vmem((512, 512), BF16),
+            vmem((2, 512, 512), BF16),
             vmem((512, 768), F32),
             vmem((512, 128), F32),
             vmem((128, 640), BF16),
@@ -724,9 +751,9 @@
             vmem((256, 512), F32),
             vmem((256, 512), F32),
             vmem((128, 128), F32),
-            dma((10,)), dma((1,)), dma((32,)), dma((32,)), dma((16,)), dma((2,)), dma((1,)), dma((2,)),
+            dma((10,)), dma((8,)), pltpu.SemaphoreType.REGULAR, dma((1,)), dma((32,)), dma((32,)), dma((16,)), dma((2,)), dma((1,)), dma((2,)),
             dma((4,)), dma((1,)), dma((8,)), dma((8,)), dma((6,)),
-            dma((10,)), dma((48,)), dma((41,)), dma((32,)), dma((10,)), dma((32,)),
+            dma((20,)), dma((48,)), dma((41,)), dma((32,)), dma((10,)), dma((32,)),
             dma((2,)), dma((1,)), dma((1,)), dma((3,)), dma((1,)),
             dma((6,)), dma((6,)), dma((3,)), dma((3,)), dma((6,)),
         ],

time: 75.8 us -> 75 us (0.989)
  no operation moved by 1% of the time
where the time goes in v4:
time: 75 us; the launch traced here: 74.9 us
  Pallas kernels  74.2 us (99%)
    pallas_call x1, Pallas kernels, per_device(): pl.pallas_call(kernel, out_shape=pltpu.VMEM((256, 512), BF16), in_specs=[...  74.2 us

profile of v4, /device:TPU:1, one launch (start us, length us, event | category | flops | bytes accessed | tf_op | source)
XLA Modules:
  0.0 74.9 jit_solution(11787006540162211252)
XLA Ops:
  0.0 74.2 %shard_map.181 = bf16[256,512]{1,0:T(8,128)(2,1)S(1)} custom-call(bf16[256,512]{1,0:T(8,128)(2,1)} %x_in.1, bf16[256,256]{1,0:T(8,128)(2,1)} %wp_in.1, bf16[256,256]{1,0:T(8,128)(2,1)} %wq_in.1, bf16[256,256]{1,0:T(8,128)(2,1)} %wk_in.1, bf16[256,256]{1,0:T(8,128)(2,1)} %wv_in.1, bf16[256,256]{1,0:T(8,128)(2,1)} %wg_in.1, bf16[256,256]{1,0:T(8,128)(2,1)} %op_in.1, ...), custom_call_target="tpu_custom_call" | custom-call | tf_op jit(solution)/shard_map/pallas_call | solution.py:701
  74.2 0.7 copy.21

commit v5 on v4

--- a/solution.py
+++ b/solution.py
@@ -29,9 +29,9 @@
     ("XR", "n", 1, 2), ("XR", "a", 3, 2), ("WT", 0), ("OB", 3), ("EARLY",), ("WT", 1),
     ("WT", 2), ("OA",), ("LATEX",), ("LATE",), ("heads",), ("ON", 1), ("level", 1), ("ON", 0),
     ("level", 2), ("OO",), ("OB2",), ("level", 3), ("level", 4), ("level", 5), ("level", 6),
-    ("level", 7), ("maps",), ("join",), ("ON", 3), ("OR", "n", 3), ("OR", "a", 1),
-    ("OR", "a", 3), ("pool",), ("ON", 2), ("OR", "n", 1), ("state",), ("finish",), ("GP",),
-    ("GD",), ("WOALL",),
+    ("level", 7), ("maps",), ("pool",), ("join",), ("ON", 3), ("OR", "n", 3), ("OR", "a", 1),
+    ("OR", "a", 3), ("ON", 2), ("OR", "n", 1), ("state",), ("finish",), ("GP",), ("GD",),
+    ("WOALL",),
 )
 
 
@@ -445,6 +445,7 @@
         depth((jnp.where(gap == 0, x2, jnp.where(gap == 2, x, z2)),), (2,))
 
     def delta_heads():
+        pl.semaphore_wait(near, 4)
         for b in (0, 1):
             @pl.when(jnp.logical_or(away, yodd != b))
             def _(b=b):
@@ -530,7 +531,6 @@
         chip_map = dot(one[:, 0:128], stc[0])
         chip_map = chip_map + jnp.concatenate([jnp.zeros((128, 128), F32), one[:, 128:256].astype(F32)], axis=1)
         stz_src[...] = chip_map.astype(BF16)
-        pl.semaphore_wait(near, 4)
         for d in (2, 1, 3):
             remote(
                 stz_src, stz.at[z], stz_ss.at[d - 1], stz_rs.at[z],

time: 75 us -> 74.9 us (level)
  no operation moved by 1% of the time
where the time goes in v5:
time: 74.9 us; the launch traced here: 74.8 us
  Pallas kernels  74.1 us (99%)
    pallas_call x1, Pallas kernels, per_device(): pl.pallas_call(kernel, out_shape=pltpu.VMEM((256, 512), BF16), in_specs=[...  74.1 us

profile of v5, /device:TPU:1, one launch (start us, length us, event | category | flops | bytes accessed | tf_op | source)
XLA Modules:
  0.0 74.8 jit_solution(5244255896501814936)
XLA Ops:
  0.0 74.1 %shard_map.181 = bf16[256,512]{1,0:T(8,128)(2,1)S(1)} custom-call(bf16[256,512]{1,0:T(8,128)(2,1)} %x_in.1, bf16[256,256]{1,0:T(8,128)(2,1)} %wp_in.1, bf16[256,256]{1,0:T(8,128)(2,1)} %wq_in.1, bf16[256,256]{1,0:T(8,128)(2,1)} %wk_in.1, bf16[256,256]{1,0:T(8,128)(2,1)} %wv_in.1, bf16[256,256]{1,0:T(8,128)(2,1)} %wg_in.1, bf16[256,256]{1,0:T(8,128)(2,1)} %op_in.1, ...), custom_call_target="tpu_custom_call" | custom-call | tf_op jit(solution)/shard_map/pallas_call | solution.py:701
  74.1 0.7 copy.21
